TPU v7x, 32 devices: a whole 2x2x4 slice. The times are simulated.
32 devices in a mesh: sp: 16 (over z, y, x), tp: 2 (over core).
Axes of the slice: x: 2, y: 2, z: 4, core: 2. Of those that a mesh axis runs over, the one named last changes fastest.
Arguments:
- projected_queries: bfloat16 [8192, 1024], P('sp', 'tp'), may hold values from -6 to 6
- projected_keys: bfloat16 [8192, 1024], P('sp', 'tp'), may hold values from -6 to 6
- projected_values: bfloat16 [8192, 1024], P('sp', 'tp'), may hold values from -6 to 6
- output_gate_values: bfloat16 [8192, 1024], P('sp', 'tp'), may hold values from -6 to 6
- write_strength_logits: bfloat16 [8192, 8], P('sp', 'tp'), may hold values from -6.5 to 3
- decay_input_logits: bfloat16 [8192, 8], P('sp', 'tp'), may hold values from -5 to 5
- head_rate_logarithm: float32 [8], P('tp'), may hold values from -8 to 2.3
- extra_log_decay: float32 [8192, 8], P('sp', 'tp'), may hold values from -0.7 to 0
- per_head_norm_gain: float32 [128], replicated, may hold values from 0.1 to 1.9
- output_matrix: bfloat16 [1024, 2048], replicated, may hold values from -0.1875 to 0.1875
- residual: bfloat16 [8192, 2048], P(('sp', 'tp')), may hold values from -6 to 6
- mixture_norm_gain: float32 [2048], replicated, may hold values from 0.1 to 1.9
- selected_expert_index: int32 [8192, 4], P(('sp', 'tp')), may hold values from 0 to 31, all different within a row; in each aligned block of 256 rows (0 to 255, 256 to 511, ...) at most 48 rows name the same one
- routing_weight: float32 [8192, 4], P(('sp', 'tp')), may hold values from 0.1 to 0.9
- routed_gate_weight: bfloat16 [32, 2048, 512], P(('sp', 'tp')), may hold values from -0.125 to 0.125
- routed_up_weight: bfloat16 [32, 2048, 512], P(('sp', 'tp')), may hold values from -0.125 to 0.125
- routed_down_weight: bfloat16 [32, 512, 2048], P(('sp', 'tp')), may hold values from -0.25 to 0.25
- common_gate_weight: bfloat16 [2048, 512], replicated, may hold values from -0.125 to 0.125
- common_up_weight: bfloat16 [2048, 512], replicated, may hold values from -0.125 to 0.125
- common_down_weight: bfloat16 [512, 2048], replicated, may hold values from -0.25 to 0.25
Outputs:
- block_out: bfloat16 [8192, 2048], P(('sp', 'tp'))
Inputs may be any that keep to these rules, and one draw needn't show every extreme that they name: `selected_expert_index`: each row names 4 different experts. Among the rows that one device holds, no expert is named more than 48 times.
All inputs are finite; a program needn't handle non-finite values.
Results may differ from a plain program's by a relative error of at most 0.008.
Values may be sent and summed in bfloat16 or wider, within the bound.
A program may use at most 192 MiB of HBM per device.

v0:
```python
import functools

import jax
import jax.numpy as jnp
from jax import lax
from jax.experimental import pallas as pl
from jax.experimental.pallas import tpu as pltpu
from jax.sharding import PartitionSpec as P

TOP_K = 4
SPAN = 64


EPS = 1e-06
HIGH = lax.Precision.HIGHEST


def exchange_kernel(axes, sizes, x_ref, o_ref, held, send_sem, recv_sem, local_sem):
    count = 1
    me = 0
    for axis, size in zip(axes, sizes):
        count *= size
        me = me * size + lax.axis_index(axis)

    def device(index):
        found = {}
        for axis, size in reversed(list(zip(axes, sizes))):
            found[axis] = lax.rem(index, size)
            index = index // size
        return found

    barrier = pltpu.get_barrier_semaphore()
    for step in range(1, count):
        pl.semaphore_signal(
            barrier,
            inc=1,
            device_id=device(lax.rem(me + step, count)),
            device_id_type=pl.DeviceIdType.MESH,
        )
    pl.semaphore_wait(barrier, count - 1)
    copies = []
    for step in range(1, count):
        peer = lax.rem(me + step, count)
        copy = pltpu.make_async_remote_copy(
            src_ref=x_ref.at[peer],
            dst_ref=o_ref.at[me],
            send_sem=send_sem.at[step],
            recv_sem=recv_sem.at[step],
            device_id=device(peer),
            device_id_type=pl.DeviceIdType.MESH,
        )
        copy.start()
        copies.append(copy)
    into = pltpu.make_async_copy(x_ref.at[me], held, local_sem)
    into.start()
    into.wait()
    out = pltpu.make_async_copy(held, o_ref.at[me], local_sem)
    out.start()
    out.wait()
    for copy in copies:
        copy.wait()


def exchange(value, axes, identity):
    sizes = tuple(lax.axis_size(axis) for axis in axes)
    count = value.shape[0]
    return pl.pallas_call(
        functools.partial(exchange_kernel, axes, sizes),
        out_shape=jax.ShapeDtypeStruct(value.shape, value.dtype),
        in_specs=[pl.BlockSpec(memory_space=pl.ANY)],
        out_specs=pl.BlockSpec(memory_space=pl.ANY),
        scratch_shapes=[
            pltpu.VMEM(value.shape[1:], value.dtype),
            pltpu.SemaphoreType.DMA((count,)),
            pltpu.SemaphoreType.DMA((count,)),
            pltpu.SemaphoreType.DMA,
        ],
        compiler_params=pltpu.CompilerParams(collective_id=identity, has_side_effects=True),
    )(value)


def shift_join(stacked, step, width):
    later = stacked[:, step:]
    joined = jnp.einsum(
        "hned,hndf->hnef", stacked[:, :-step], later[:, :, :width], precision=HIGH
    )
    joined = jnp.concatenate(
        [joined[:, :, :width], joined[:, :, width:] + later[:, :, width:]], axis=2
    )
    return jnp.concatenate([stacked[:, :step], joined], axis=1)


def inclusive(stacked, width):
    step = 1
    while step < stacked.shape[1]:
        stacked = shift_join(stacked, step, width)
        step *= 2
    return stacked


def starts_of(total):
    heads, _, width = total.shape
    count = lax.axis_size("sp")
    parts = count // heads
    mapping = jnp.repeat(total[:, :width], parts, axis=0)
    carried = total[:, width:].reshape(count, width // parts, width)
    arrived = exchange(jnp.concatenate([mapping, carried], axis=1), ("sp",), 0)
    joined = inclusive(arrived[None], width)[0, :, width:]
    before = jnp.concatenate([jnp.zeros_like(joined[:1]), joined[:-1]], axis=0)
    return exchange(before, ("sp",), 1).reshape(heads, width, width)


def invert_kernel(n_ref, x_ref):
    span = n_ref.shape[-1]
    row = lax.broadcasted_iota(jnp.int32, (span, span), 0)
    column = lax.broadcasted_iota(jnp.int32, (span, span), 1)
    one = (row == column).astype(jnp.float32)
    strict = [n_ref[i] for i in range(n_ref.shape[0])]
    found = None
    size = 1
    while size < span:
        pair = (row // size) - (column // size)
        mask = ((row // size) % 2 == 1) & (pair == 1)
        below = [jnp.where(mask, part, 0.0) for part in strict]
        if found is None:
            found = [one - part for part in below]
        else:
            inner = [
                jnp.dot(x, part, precision=HIGH, preferred_element_type=jnp.float32)
                for x, part in zip(found, below)
            ]
            found = [
                x - jnp.dot(y, x, precision=HIGH, preferred_element_type=jnp.float32)
                for x, y in zip(found, inner)
            ]
        size *= 2
    for i, x in enumerate(found):
        x_ref[i] = x


def invert_unit_lower(strict):
    number, span, _ = strict.shape
    group = 8 if number % 8 == 0 else 1
    spec = pl.BlockSpec((group, span, span), lambda i: (i, 0, 0))
    return pl.pallas_call(
        invert_kernel,
        grid=(number // group,),
        out_shape=jax.ShapeDtypeStruct(strict.shape, jnp.float32),
        in_specs=[spec],
        out_specs=spec,
    )(strict)


def unit_heads(raw, heads):
    active = jax.nn.silu(raw.astype(jnp.float32)).reshape(raw.shape[0], heads, -1)
    return active * lax.rsqrt(jnp.sum(active * active, axis=-1, keepdims=True) + EPS)


def prepare_inputs(
    projected_queries,
    projected_keys,
    projected_values,
    write_strength_logits,
    decay_input_logits,
    head_rate_logarithm,
    extra_log_decay,
):
    heads = head_rate_logarithm.shape[0]
    queries = unit_heads(projected_queries, heads)
    keys = unit_heads(projected_keys, heads)
    values = jax.nn.silu(projected_values.astype(jnp.float32)).reshape(
        projected_values.shape[0], heads, -1
    )
    beta = jax.nn.sigmoid(write_strength_logits.astype(jnp.float32))
    decay_logarithm = extra_log_decay - jnp.exp(head_rate_logarithm)[None, :] * jax.nn.softplus(
        decay_input_logits.astype(jnp.float32) - 6.0
    )
    return (queries, keys, values, beta, decay_logarithm)


def block_terms(queries, keys, values, beta, decay_logarithm):
    length, heads, width = queries.shape
    number = length // SPAN

    def split(array):
        return jnp.moveaxis(array.reshape(number, SPAN, heads, -1), 2, 0)

    q_blocks = split(queries)
    k_blocks = split(keys)
    v_blocks = split(values)
    b_blocks = split(beta[..., None])[..., 0]
    g_cumul = jnp.cumsum(split(decay_logarithm[..., None])[..., 0], axis=-1)
    place = jnp.arange(SPAN)
    causal = place[:, None] >= place[None, :]
    strict = place[:, None] > place[None, :]
    spread = jnp.where(causal, g_cumul[..., :, None] - g_cumul[..., None, :], 0.0)
    decay = jnp.where(causal, jnp.exp(spread), 0.0)
    k_beta = k_blocks * b_blocks[..., None]
    inner = jnp.einsum("hncd,hnsd->hncs", k_beta, k_blocks, precision=HIGH)
    lower = jnp.where(strict, inner * decay, 0.0)
    inverse = invert_unit_lower(lower.reshape(heads * number, SPAN, SPAN)).reshape(lower.shape)
    right = jnp.concatenate(
        [k_beta * jnp.exp(g_cumul)[..., None], v_blocks * b_blocks[..., None]], axis=-1
    )
    solved = jnp.einsum("hncs,hnsd->hncd", inverse, right, precision=HIGH)
    scores = jnp.einsum("hncd,hnsd->hncs", q_blocks, k_blocks, precision=HIGH) * decay
    q_decayed = q_blocks * jnp.exp(g_cumul)[..., None]
    log_last = g_cumul[..., -1]
    k_decayed = k_blocks * jnp.exp(log_last[..., None] - g_cumul)[..., None]
    return (q_decayed, scores, solved, k_decayed, log_last)


def mix_heads(terms):
    q_decayed, scores, solved, k_decayed, log_last = terms
    heads, number, span, width = q_decayed.shape
    maps = jnp.einsum("hnce,hncd->hned", solved, k_decayed, precision=HIGH)
    identity = jnp.eye(width, dtype=jnp.float32)
    maps = jnp.concatenate(
        [
            identity * jnp.exp(log_last)[..., None, None] - maps[:, :, :width],
            maps[:, :, width:],
        ],
        axis=2,
    )
    joined = inclusive(maps, width)
    start = starts_of(joined[:, -1])
    mixed = jnp.einsum("hncs,hnsd->hncd", scores, solved, precision=HIGH)
    reads = q_decayed - mixed[..., :width]
    later = jnp.einsum("hed,hndf->hnef", start, joined[:, :-1, :width], precision=HIGH)
    states = jnp.concatenate([start[:, None], later + joined[:, :-1, width:]], axis=1)
    result = mixed[..., width:] + jnp.einsum("hncd,hned->hnce", reads, states, precision=HIGH)
    return result.transpose(1, 2, 0, 3).reshape(number * span, heads, width)


def finish(head_mix, output_gate_values, per_head_norm_gain):
    length, heads, width = head_mix.shape
    scaled = head_mix * lax.rsqrt(jnp.mean(head_mix * head_mix, axis=-1, keepdims=True) + EPS)
    gated = (
        scaled
        * per_head_norm_gain
        * jax.nn.silu(output_gate_values.astype(jnp.float32).reshape(length, heads, width))
    )
    return gated.reshape(length, heads * width).astype(jnp.bfloat16)


def normalize(stream, gain):
    wide = stream.astype(jnp.float32)
    return (wide * lax.rsqrt(jnp.mean(wide * wide, axis=-1, keepdims=True) + EPS) * gain).astype(
        jnp.bfloat16
    )


def feed_forward(rows, w_gate, w_up, w_down):
    hidden = jax.nn.silu(jnp.dot(rows, w_gate, preferred_element_type=jnp.float32))
    hidden = (hidden * jnp.dot(rows, w_up, preferred_element_type=jnp.float32)).astype(jnp.bfloat16)
    return jnp.dot(hidden, w_down, preferred_element_type=jnp.float32)


def shards(
    projected_queries,
    projected_keys,
    projected_values,
    output_gate_values,
    write_strength_logits,
    decay_input_logits,
    head_rate_logarithm,
    extra_log_decay,
    per_head_norm_gain,
    output_matrix,
    residual,
    mixture_norm_gain,
    selected_expert_index,
    routing_weight,
    routed_gate_weight,
    routed_up_weight,
    routed_down_weight,
    common_gate_weight,
    common_up_weight,
    common_down_weight,
):
    prepared_inputs = prepare_inputs(
        projected_queries,
        projected_keys,
        projected_values,
        write_strength_logits,
        decay_input_logits,
        head_rate_logarithm,
        extra_log_decay,
    )
    terms = block_terms(*prepared_inputs)
    heads_out = finish(mix_heads(terms), output_gate_values, per_head_norm_gain)
    token_heads = lax.all_to_all(heads_out, "tp", split_axis=0, concat_axis=1, tiled=True)
    projected = jnp.dot(token_heads, output_matrix, preferred_element_type=jnp.float32)
    attended = (residual.astype(jnp.float32) + projected).astype(jnp.bfloat16)
    normed = normalize(attended, mixture_norm_gain)
    length = normed.shape[0]
    experts = lax.axis_size("sp") * lax.axis_size("tp")
    room = max(2, length * TOP_K * 3 // (2 * experts))
    chosen = selected_expert_index[:, :, None] == jnp.arange(experts, dtype=jnp.int32)
    named = jnp.any(chosen, axis=1)
    weight = jnp.sum(jnp.where(chosen, routing_weight[:, :, None], 0.0), axis=1)
    place = jnp.arange(length, dtype=jnp.int32)
    earlier = (place[:, None] > place[None, :]).astype(jnp.bfloat16)
    slot = jnp.dot(earlier, named.astype(jnp.bfloat16), preferred_element_type=jnp.float32)
    slot = jnp.where(named, slot.astype(jnp.int32), room)
    picked = slot.T[:, None, :] == jnp.arange(room, dtype=jnp.int32)[None, :, None]
    picked = picked.reshape(experts * room, length)
    outgoing = jnp.dot(
        picked.astype(jnp.bfloat16), normed, preferred_element_type=jnp.float32
    ).astype(jnp.bfloat16)
    arrived = exchange(outgoing.reshape(experts, room, -1), ("sp", "tp"), 2)
    flat = arrived.reshape(-1, arrived.shape[-1])
    result = feed_forward(
        flat, routed_gate_weight[0], routed_up_weight[0], routed_down_weight[0]
    ).astype(jnp.bfloat16)
    back = exchange(result.reshape(arrived.shape), ("sp", "tp"), 3).reshape(experts * room, -1)
    high = weight.astype(jnp.bfloat16)
    low = (weight - high.astype(jnp.float32)).astype(jnp.bfloat16)

    def weighted(part):
        spread = jnp.broadcast_to(part.T[:, None, :], (experts, room, length))
        spread = jnp.where(picked, spread.reshape(experts * room, length), 0)
        return jnp.einsum("pt,pd->td", spread, back, preferred_element_type=jnp.float32)

    routed = weighted(high) + weighted(low)
    shared = feed_forward(normed, common_gate_weight, common_up_weight, common_down_weight)
    return (attended.astype(jnp.float32) + shared + routed).astype(jnp.bfloat16)


def solution(mesh):
    return jax.shard_map(
        shards,
        mesh=mesh,
        in_specs=(
            P("sp", "tp"),
            P("sp", "tp"),
            P("sp", "tp"),
            P("sp", "tp"),
            P("sp", "tp"),
            P("sp", "tp"),
            P("tp"),
            P("sp", "tp"),
            P(),
            P(),
            P(("sp", "tp"), None),
            P(),
            P(("sp", "tp"), None),
            P(("sp", "tp"), None),
            P(("sp", "tp"), None, None),
            P(("sp", "tp"), None, None),
            P(("sp", "tp"), None, None),
            P(),
            P(),
            P(),
        ),
        out_specs=P(("sp", "tp"), None),
        check_vma=False,
    )
```

profile of v0, /device:TPU:15, one launch (start us, length us, event | category | flops | bytes accessed | tf_op | source)
XLA Modules:
  0.0 525.5 jit_solution(12127107603031870800)
XLA Ops:
  2.8 2.4 fusion.122
  10.3 2.3 convert_multiply_fusion.3
  12.5 2.6 reshape_reshape.3
  15.1 3.6 fusion.46
  18.8 11.0 %shard_map.190 = f32[32,64,64]{2,1,0:T(8,128)} custom-call(f32[32,64,64]{2,1,0:T(8,128)} %bitcast.170), custom_call_target="tpu_custom_call" | custom-call | tf_op jit(solution)/shard_map/pallas_call | solution.py:145
  29.7 2.3 multiply_multiply_fusion
  32.0 1.9 fusion.14
  35.3 7.9 %fusion.72 = f32[4,8,256,128]{3,2,1,0:T(8,128)S(1)} fusion(f32[4,8,64,256]{3,2,1,0:T(8,128)S(1)} %fusion.14, f32[8,64,4,128]{3,2,1,0:T(4,128)S(1)} %reshape.174, f32[4,8,64]{2,1,0:T(8,128)S(1)} %get-tuple-element.21, f32[8,64,4]{1,0,2:T(8,128)S(1)} %copy.47), kind=kOutput, calls=%fused_computation.114 | convolution fusion | flops 805830656 | bytes 7356416 | tf_op jit(solution)/shard_map/hnce,hncd->hned/dot_general | solution.py:216
  43.7 4.3 fusion.2
  49.0 3.3 fusion.29
  53.4 2.0 fusion.4
  58.1 35.5 %shard_map.191 = f32[16,160,128]{2,1,0:T(8,128)} custom-call(f32[16,160,128]{2,1,0:T(8,128)} %pad_maximum_fusion.7.x_ref), custom_call_target="tpu_custom_call" | custom-call | tf_op jit(solution)/shard_map/pallas_call | solution.py:67
  93.6 2.9 convolution_bitcast_fusion.2
  104.0 2.3 fusion.5
  107.1 9.6 %shard_map.192 = f32[16,32,128]{2,1,0:T(8,128)} custom-call(f32[16,32,128]{2,1,0:T(8,128)} %concatenate.73.x_ref), custom_call_target="tpu_custom_call" | custom-call | tf_op jit(solution)/shard_map/pallas_call | solution.py:67
  116.6 2.7 fusion.121
  119.4 2.6 mul.177
  125.6 2.5 reshape.173
  128.2 3.5 convolution_multiply_fusion.1
  133.7 3.9 slice_add_fusion
  137.6 4.3 multiply_reduce_fusion
  144.0 5.5 %all_to_all.19 = bf16[2,256,512]{1,2,0:T(8,128)(2,1)S(1)} all-to-all(bf16[2,256,512]{1,2,0:T(8,128)(2,1)S(1)} %copy.55), channel_id=1, replica_groups=mesh['sp'=16,'tp'=2] {'tp'}, dimensions={0} | all-to-all | bytes 1048576 | tf_op jit(solution)/shard_map/all_to_all | solution.py:292
  149.5 3.9 fusion.11
  154.1 3.2 fusion.119
  157.3 4.6 convolution_convert_fusion
  161.8 165.7 %shard_map.193 = bf16[32,48,2048]{2,1,0:T(8,128)(2,1)} custom-call(bf16[32,48,2048]{2,1,0:T(8,128)(2,1)} %bitcast.155), custom_call_target="tpu_custom_call" | custom-call | tf_op jit(solution)/shard_map/pallas_call | solution.py:67
  327.6 8.5 %fusion.24 = f32[1536,512]{1,0:T(8,128)} fusion(bf16[1536,2048]{1,0:T(8,128)(2,1)} %bitcast.159, bf16[1,2048,512]{2,1,0:T(8,128)(2,1)} %param.34), kind=kOutput, calls=%fused_computation.44 | convolution fusion | flops 3221225472 | bytes 11534336 | tf_op jit(solution)/shard_map/dot_general | solution.py:254
  336.0 12.0 %convolution_convert_fusion.1 = bf16[1536,2048]{1,0:T(8,128)(2,1)} fusion(bf16[1,512,2048]{2,1,0:T(8,128)(2,1)S(1)} %copy-done, bf16[1536,2048]{1,0:T(8,128)(2,1)} %bitcast.160, f32[1536,512]{1,0:T(8,128)} %fusion.24, bf16[1,2048,512]{2,1,0:T(8,128)(2,1)} %param.35), kind=kOutput, calls=%fused_computation.1 | convolution fusion | flops 6450315264 | bytes 19922944 | tf_op jit(solution)/shard_map/dot_general | solution.py:256
  348.1 163.7 %shard_map.194 = bf16[32,48,2048]{2,1,0:T(8,128)(2,1)} custom-call(bf16[32,48,2048]{2,1,0:T(8,128)(2,1)} %bitcast.161), custom_call_target="tpu_custom_call" | custom-call | tf_op jit(solution)/shard_map/pallas_call | solution.py:67
  511.9 4.7 convolution_bitcast_fusion
  516.6 3.2 fusion.8
  519.8 5.5 %fusion.9 = bf16[256,2048]{1,0:T(8,128)(2,1)} fusion(f32[256,2048]{1,0:T(8,128)} %fusion.8, bf16[512,2048]{1,0:T(8,128)(2,1)} %param.39, bf16[256,2048]{1,0:T(8,128)(2,1)S(1)} %get-tuple-element.28, bf16[2048,512]{1,0:T(8,128)(2,1)} %param.38, f32[256,512]{1,0:T(8,128)} %fusion.119, f32[2048]{0:T(1024)S(1)} %copy-done.19, f32[256]{0:T(256)S(1)} %add_rsqrt_fusion.3), kind=kOutput, calls=%fused_computation.28 | convolution fusion | flops 1078722560 | bytes 8922112 | tf_op jit(solution)/shard_map/dot_general | solution.py:256
  (108 shorter events, 30.6 us)
Async XLA Ops:
  0.0 336.0 %copy-start = (bf16[1,512,2048]{2,1,0:T(8,128)(2,1)S(1)}, bf16[1,512,2048]{2,1,0:T(8,128)(2,1)}, u32[]{:S(2)}) copy-start(bf16[1,512,2048]{2,1,0:T(8,128)(2,1)} %param.36) | copy-start | bytes 6291460
  6.5 3.6 copy-start.20
  29.7 2.3 copy-start.15
  34.0 1.3 copy-start.2
  52.4 1.0 copy-start.13
  52.8 2.5 copy-start.4
  52.8 2.5 copy-start.11
  55.6 1.0 copy-start.6
  55.6 1.4 copy-start.8
  101.2 1.2 copy-start.14
  101.2 1.5 copy-start.9
  101.3 2.0 copy-start.12
  101.3 2.4 copy-start.5
  101.3 2.7 copy-start.7
  128.2 3.5 copy-start.3
  131.7 2.0 copy-start.16
  133.6 4.0 copy-start.10
  141.9 0.9 copy-start.22
  142.1 1.3 copy-start.17
  149.5 3.9 copy-start.18
  149.5 4.5 copy-start.19
  348.1 163.7 %copy-start.21 = (f32[256,4]{0,1:T(4,128)S(1)}, f32[256,4]{0,1:T(4,128)}, u32[]{:S(2)}) copy-start(f32[256,4]{0,1:T(4,128)} %param.33) | copy-start | bytes 12292
  511.8 4.8 copy-start.1
where the time goes:
time: 531 us; the launch traced here: 525 us
  Pallas kernels  386 us (73%)
  matrix products  88.4 us (17%)
  other arithmetic  23.5 us (4%)
  local copies, waits for them, and re-layouts  21.6 us (4%)
  blocking collectives  5.53 us (1%)
    pallas_call x4, Pallas kernels, exchange(): pl.pallas_call(functools.partial(exchange_kernel, axes, sizes), out_shape...  375 us
    dot_general x2, matrix products, feed_forward(): return jnp.dot(hidden, w_down, preferred_element_type=jnp.float32)  17.5 us
    dot_general x7, matrix products, shift_join(): jnp.einsum('hned,hndf->hnef', stacked[:, :-step], later[:, :, :width], pr...  15.6 us
    dot_general x2, matrix products, feed_forward(): jnp.dot(rows, w_gate, preferred_element_type=jnp.float32)  11.7 us
    pallas_call x1, Pallas kernels, invert_unit_lower(): pl.pallas_call(invert_kernel, grid=(number // group,), out_shape=jax.Shap...  11 us

commit v1 on v0

--- a/solution.py
+++ b/solution.py
@@ -250,10 +250,505 @@
     )
 
 
-def feed_forward(rows, w_gate, w_up, w_down):
-    hidden = jax.nn.silu(jnp.dot(rows, w_gate, preferred_element_type=jnp.float32))
-    hidden = (hidden * jnp.dot(rows, w_up, preferred_element_type=jnp.float32)).astype(jnp.bfloat16)
-    return jnp.dot(hidden, w_down, preferred_element_type=jnp.float32)
+def lookup(table, index):
+    found = table[0]
+    for place in range(1, len(table)):
+        found = jnp.where(index == place, table[place], found)
+    return found
+
+
+def relay_orders(count):
+    arrive, leave, when = [], [], []
+    for me in range(count):
+        others = [s for s in range(count) if s != me]
+        middle = (count - 1) / 2
+        arrive.append(sorted(others, key=lambda s: (abs(s - me), abs(s - middle))))
+
+        def key(d):
+            reach = (count - 1 - d) if me > d else d
+            return (reach, reach - abs(me - d))
+
+        order = sorted(others, key=key)
+        leave.append(order)
+        steps, latest = [], 0
+        for d in order:
+            latest = max(latest, arrive[me].index(d) + 1)
+            steps.append(latest)
+        when.append(steps)
+    return arrive, leave, when
+
+
+def experts_kernel(
+    count,
+    ring,
+    room,
+    pieces,
+    x_ref,
+    attended_ref,
+    info_ref,
+    gate_hbm,
+    up_hbm,
+    down_hbm,
+    common_gate_hbm,
+    common_up_hbm,
+    common_down_hbm,
+    out_ref,
+    held,
+    tables,
+    outbox,
+    inbox,
+    backbox,
+    relay,
+    part,
+    total,
+    hidden,
+    picks,
+    shares,
+    gate,
+    up,
+    down,
+    common_gate,
+    common_up,
+    common_down,
+    weight_sem,
+    info_send,
+    info_recv,
+    hold_send,
+    hold_recv,
+    go_send,
+    go_recv,
+    back_send,
+    back_recv,
+    relay_send,
+    relay_recv,
+):
+    length, width = x_ref.shape
+    tp_size = lax.axis_size("tp")
+    inner = lax.axis_size("sp") // count
+    sp = lax.axis_index("sp")
+    outer = sp // inner
+    mine = lax.rem(sp, inner) * tp_size + lax.axis_index("tp")
+    MESH = pl.DeviceIdType.MESH
+    piece = length // pieces
+    slots = ring * room
+    arrive, leave, when = relay_orders(count)
+
+    def device(o, i):
+        return {"sp": o * inner + i // tp_size, "tp": lax.rem(i, tp_size)}
+
+    loads = []
+    for n, (src, dst) in enumerate(
+        (
+            (common_gate_hbm, common_gate),
+            (common_up_hbm, common_up),
+            (common_down_hbm, common_down),
+            (gate_hbm, gate),
+            (up_hbm, up),
+            (down_hbm, down),
+        )
+    ):
+        load = pltpu.make_async_copy(src, dst, weight_sem.at[n])
+        load.start()
+        loads.append(load)
+
+    barrier = pltpu.get_barrier_semaphore()
+    for step in range(1, count):
+        pl.semaphore_signal(
+            barrier, inc=1, device_id=device(lax.rem(outer + step, count), mine), device_id_type=MESH
+        )
+    for step in range(1, ring):
+        pl.semaphore_signal(
+            barrier, inc=1, device_id=device(outer, lax.rem(mine + step, ring)), device_id_type=MESH
+        )
+    pl.semaphore_wait(barrier, count + ring - 2)
+
+    def remote(src, dst, send, recv, o, i):
+        return pltpu.make_async_remote_copy(
+            src_ref=src,
+            dst_ref=dst,
+            send_sem=send,
+            recv_sem=recv,
+            device_id=device(o, i),
+            device_id_type=MESH,
+        )
+
+    info_copies = []
+    for step in range(1, count):
+        peer = lax.rem(outer + step, count)
+        copy = remote(
+            info_ref.at[peer], tables.at[outer], info_send.at[step], info_recv.at[step], peer, mine
+        )
+        copy.start()
+        info_copies.append(copy)
+
+    def rows_of(c, size):
+        return pl.ds(c * size, size)
+
+    has_right = outer + 1 < count
+    has_left = outer > 0
+
+    def own_copy(c, right):
+        rows = rows_of(c, piece)
+        target = outer + 1 if right else outer - 1
+        sem = hold_send.at[count, c] if right else hold_send.at[outer, c]
+        return remote(x_ref.at[rows], held.at[outer, rows], sem, hold_recv.at[outer, c], target, mine)
+
+    for c in range(pieces):
+
+        @pl.when(has_right)
+        def _():
+            own_copy(c, True).start()
+
+        @pl.when(has_left)
+        def _():
+            own_copy(c, False).start()
+
+    held[outer] = x_ref[...]
+    tables[outer] = info_ref[outer]
+
+    def matched(source):
+        slot = tables[source, :ring, :]
+        place = lax.broadcasted_iota(jnp.int32, (ring, room, length), 1).astype(jnp.float32)
+        return slot[:, None, :] == place
+
+    def go_copy(j, source, step):
+        peer = lax.rem(mine + step, ring)
+        rows = pl.ds(pl.multiple_of(peer * room, room), room)
+        mine_rows = pl.ds(pl.multiple_of(mine * room, room), room)
+        return remote(
+            outbox.at[source, rows],
+            inbox.at[source, mine_rows],
+            go_send.at[j, step],
+            go_recv.at[j, step],
+            outer,
+            peer,
+        )
+
+    def back_copy(j, source, step):
+        peer = lax.rem(mine + step, ring)
+        rows = pl.ds(pl.multiple_of(peer * room, room), room)
+        mine_rows = pl.ds(pl.multiple_of(mine * room, room), room)
+        return remote(
+            inbox.at[source, rows],
+            backbox.at[source, mine_rows],
+            back_send.at[j, step],
+            back_recv.at[j, step],
+            outer,
+            peer,
+        )
+
+    def spread(j, source):
+        picks[...] = (
+            jnp.where(matched(source), 1.0, 0.0).reshape(slots, length).astype(jnp.bfloat16)
+        )
+        tile = min(512, width)
+
+        def body(n, carry):
+            cols = pl.ds(pl.multiple_of(n * tile, tile), tile)
+            outbox[source, :, cols] = jnp.dot(
+                picks[...], held[source, :, cols], preferred_element_type=jnp.float32
+            ).astype(jnp.bfloat16)
+            return carry
+
+        lax.fori_loop(0, width // tile, body, 0)
+        for step in range(1, ring):
+            go_copy(j, source, step).start()
+        mine_rows = pl.ds(pl.multiple_of(mine * room, room), room)
+        inbox[source, mine_rows, :] = outbox[source, mine_rows, :]
+
+    def feed(rows_ref, count_rows, w_gate, w_up, w_down, store):
+        inside = w_gate.shape[1]
+        tile = min(256, inside)
+
+        def first(n, carry):
+            cols = pl.ds(pl.multiple_of(n * tile, tile), tile)
+            rows = rows_ref[...]
+            gated = jnp.dot(rows, w_gate[:, cols], preferred_element_type=jnp.float32)
+            lifted = jnp.dot(rows, w_up[:, cols], preferred_element_type=jnp.float32)
+            hidden[pl.ds(0, count_rows), cols] = (gated * jax.nn.sigmoid(gated) * lifted).astype(
+                jnp.bfloat16
+            )
+            return carry
+
+        lax.fori_loop(0, inside // tile, first, 0)
+        wide = min(512, width)
+
+        def second(n, carry):
+            cols = pl.ds(pl.multiple_of(n * wide, wide), wide)
+            store(
+                cols,
+                jnp.dot(
+                    hidden[pl.ds(0, count_rows), :],
+                    w_down[:, cols],
+                    preferred_element_type=jnp.float32,
+                ),
+            )
+            return carry
+
+        lax.fori_loop(0, width // wide, second, 0)
+
+    def serve(j, source):
+        for step in range(1, ring):
+            go_copy(j, source, step).wait_recv()
+
+        def store(cols, value):
+            inbox[source, :, cols] = value.astype(jnp.bfloat16)
+
+        feed(inbox.at[source], slots, gate, up, down, store)
+
+    def send_back(j, source):
+        for step in range(1, ring):
+            back_copy(j, source, step).start()
+        mine_rows = pl.ds(pl.multiple_of(mine * room, room), room)
+        backbox[source, mine_rows, :] = inbox[source, mine_rows, :]
+
+    def combine(j, source, store):
+        weight = tables[source, ring:, :]
+        spread_weight = jnp.where(matched(source), weight[:, None, :], 0.0).reshape(slots, length)
+        turned = spread_weight.T
+        high = turned.astype(jnp.bfloat16)
+        shares[0] = high
+        shares[1] = (turned - high.astype(jnp.float32)).astype(jnp.bfloat16)
+        for step in range(1, ring):
+            back_copy(j, source, step).wait_recv()
+        tile = min(512, width)
+
+        def body(n, carry):
+            cols = pl.ds(pl.multiple_of(n * tile, tile), tile)
+            rows = backbox[source, :, cols]
+            store(
+                cols,
+                jnp.dot(shares[0], rows, preferred_element_type=jnp.float32)
+                + jnp.dot(shares[1], rows, preferred_element_type=jnp.float32),
+            )
+            return carry
+
+        lax.fori_loop(0, width // tile, body, 0)
+
+    def forward_copy(source, c):
+        rows = rows_of(c, piece)
+        target = jnp.where(source < outer, outer + 1, outer - 1)
+        return remote(
+            held.at[source, rows],
+            held.at[source, rows],
+            hold_send.at[jnp.where(source < outer, source, source), c],
+            hold_recv.at[source, c],
+            target,
+            mine,
+        )
+
+    def goes_on(source):
+        return ((source < outer) & has_right) | ((source > outer) & has_left)
+
+    def receive(source):
+        for c in range(pieces):
+            forward_copy(source, c).wait_recv()
+
+            @pl.when(goes_on(source))
+            def _():
+                forward_copy(source, c).start()
+
+    def relay_copy(dest, c):
+        rows = rows_of(c, piece)
+        leftward = dest < outer
+        target = jnp.where(leftward, outer - 1, outer + 1)
+        landing = jnp.where(leftward & (target == dest), count, dest)
+        return remote(
+            relay.at[dest, rows],
+            relay.at[landing, rows],
+            relay_send.at[dest, c],
+            relay_recv.at[landing, c],
+            target,
+            mine,
+        )
+
+    def landed(place, c):
+        rows = rows_of(c, piece)
+        return remote(
+            relay.at[place, rows],
+            relay.at[place, rows],
+            relay_send.at[0, c],
+            relay_recv.at[place, c],
+            lax.rem(outer + 1, count),
+            mine,
+        )
+
+    def pass_on(dest):
+        upstream = ((dest < outer) & has_right) | ((dest > outer) & has_left)
+        for c in range(pieces):
+            rows = rows_of(c, piece)
+
+            @pl.when(upstream)
+            def _():
+                landed(dest, c).wait_recv()
+                relay[dest, rows, :] = (
+                    relay[dest, rows, :].astype(jnp.float32) + part[dest, rows, :]
+                ).astype(jnp.bfloat16)
+
+            @pl.when(jnp.logical_not(upstream))
+            def _():
+                relay[dest, rows, :] = part[dest, rows, :].astype(jnp.bfloat16)
+
+            relay_copy(dest, c).start()
+
+    order = [outer] + [lookup([arrive[m][j] for m in range(count)], outer) for j in range(count - 1)]
+    drain = [lookup([leave[m][j] for m in range(count)], outer) for j in range(count - 1)]
+
+    spread(0, outer)
+    for load in loads[:3]:
+        load.wait()
+
+    def keep(cols, value):
+        total[:, cols] = attended_ref[:, cols].astype(jnp.float32) + value
+
+    feed(x_ref, length, common_gate, common_up, common_down, keep)
+    for copy in info_copies:
+        copy.wait_recv()
+
+    def store_part(source):
+        def store(cols, value):
+            part[source, :, cols] = value
+
+        return store
+
+    def collect(j):
+        combine(j, order[j], store_part(order[j]))
+        for k in range(count - 1):
+            places = [when[m][k] for m in range(count)]
+            if j in places:
+                if all(p == j for p in places):
+                    pass_on(drain[k])
+                else:
+
+                    @pl.when(lookup([int(p == j) for p in places], outer) == 1)
+                    def _():
+                        pass_on(drain[k])
+
+    for j in range(1, count):
+        if j == 2:
+            serve(1, order[1])
+            send_back(1, order[1])
+        receive(order[j])
+        spread(j, order[j])
+        if j == 1:
+            for load in loads[3:]:
+                load.wait()
+            serve(0, order[0])
+        if j > 2:
+            serve(j - 1, order[j - 1])
+            send_back(j - 1, order[j - 1])
+            collect(j - 2)
+    last = count - 1
+    if last == 1 or last > 1:
+        serve(last, order[last])
+        send_back(last, order[last])
+    send_back(0, order[0])
+    if last > 1:
+        collect(last - 1)
+    collect(last)
+
+    def add(cols, value):
+        total[:, cols] += value
+
+    combine(0, order[0], add)
+    for side, place in ((has_left, outer), (has_right, count)):
+        for c in range(pieces):
+            rows = rows_of(c, piece)
+
+            @pl.when(side)
+            def _():
+                landed(place, c).wait_recv()
+                total[rows, :] += relay[place, rows, :].astype(jnp.float32)
+
+    out_ref[...] = total[...].astype(jnp.bfloat16)
+
+    for copy in info_copies:
+        copy.wait_send()
+    for c in range(pieces):
+
+        @pl.when(has_right)
+        def _():
+            own_copy(c, True).wait_send()
+
+        @pl.when(has_left)
+        def _():
+            own_copy(c, False).wait_send()
+
+    for j in range(count):
+        if j > 0:
+            for c in range(pieces):
+
+                @pl.when(goes_on(order[j]))
+                def _():
+                    forward_copy(order[j], c).wait_send()
+
+                relay_copy(order[j], c).wait_send()
+        for step in range(1, ring):
+            go_copy(j, order[j], step).wait_send()
+            back_copy(j, order[j], step).wait_send()
+
+
+def outer_size(size):
+    bits = size.bit_length() - 1
+    return 1 << -(-bits // 3)
+
+
+def experts_part(
+    normed,
+    attended,
+    info,
+    count,
+    ring,
+    room,
+    weights,
+    identity,
+):
+    length, width = normed.shape
+    inside = weights[0].shape[1]
+    shared = weights[3].shape[1]
+    pieces = 4
+    slots = ring * room
+    bf16 = jnp.bfloat16
+    vmem = pl.BlockSpec(memory_space=pltpu.VMEM)
+    anywhere = pl.BlockSpec(memory_space=pl.ANY)
+    dma = pltpu.SemaphoreType.DMA
+    return pl.pallas_call(
+        functools.partial(experts_kernel, count, ring, room, pieces),
+        name="experts",
+        out_shape=jax.ShapeDtypeStruct((length, width), bf16),
+        in_specs=[vmem] * 3 + [anywhere] * 6,
+        out_specs=vmem,
+        scratch_shapes=[
+            pltpu.VMEM((count, length, width), bf16),
+            pltpu.VMEM((count,) + info.shape[1:], jnp.float32),
+            pltpu.VMEM((count, slots, width), bf16),
+            pltpu.VMEM((count, slots, width), bf16),
+            pltpu.VMEM((count, slots, width), bf16),
+            pltpu.VMEM((count + 1, length, width), bf16),
+            pltpu.VMEM((count, length, width), jnp.float32),
+            pltpu.VMEM((length, width), jnp.float32),
+            pltpu.VMEM((max(slots, length), max(inside, shared)), bf16),
+            pltpu.VMEM((slots, length), bf16),
+            pltpu.VMEM((2, length, slots), bf16),
+        ]
+        + [pltpu.VMEM(w.shape, w.dtype) for w in weights]
+        + [
+            dma((6,)),
+            dma((count,)),
+            dma((count,)),
+            dma((count + 1, pieces)),
+            dma((count, pieces)),
+            dma((count, ring)),
+            dma((count, ring)),
+            dma((count, ring)),
+            dma((count, ring)),
+            dma((count, pieces)),
+            dma((count + 1, pieces)),
+        ],
+        compiler_params=pltpu.CompilerParams(
+            collective_id=identity, has_side_effects=True, vmem_limit_bytes=67043328
+        ),
+    )(normed, attended, info, *weights)
 
 
 def shards(
@@ -294,37 +789,32 @@
     attended = (residual.astype(jnp.float32) + projected).astype(jnp.bfloat16)
     normed = normalize(attended, mixture_norm_gain)
     length = normed.shape[0]
-    experts = lax.axis_size("sp") * lax.axis_size("tp")
+    tp_size = lax.axis_size("tp")
+    sp_size = lax.axis_size("sp")
+    experts = sp_size * tp_size
+    count = outer_size(sp_size)
+    ring = experts // count
     room = max(2, length * TOP_K * 3 // (2 * experts))
+    room = -(-room // 16) * 16
     chosen = selected_expert_index[:, :, None] == jnp.arange(experts, dtype=jnp.int32)
     named = jnp.any(chosen, axis=1)
     weight = jnp.sum(jnp.where(chosen, routing_weight[:, :, None], 0.0), axis=1)
     place = jnp.arange(length, dtype=jnp.int32)
     earlier = (place[:, None] > place[None, :]).astype(jnp.bfloat16)
     slot = jnp.dot(earlier, named.astype(jnp.bfloat16), preferred_element_type=jnp.float32)
-    slot = jnp.where(named, slot.astype(jnp.int32), room)
-    picked = slot.T[:, None, :] == jnp.arange(room, dtype=jnp.int32)[None, :, None]
-    picked = picked.reshape(experts * room, length)
-    outgoing = jnp.dot(
-        picked.astype(jnp.bfloat16), normed, preferred_element_type=jnp.float32
-    ).astype(jnp.bfloat16)
-    arrived = exchange(outgoing.reshape(experts, room, -1), ("sp", "tp"), 2)
-    flat = arrived.reshape(-1, arrived.shape[-1])
-    result = feed_forward(
-        flat, routed_gate_weight[0], routed_up_weight[0], routed_down_weight[0]
-    ).astype(jnp.bfloat16)
-    back = exchange(result.reshape(arrived.shape), ("sp", "tp"), 3).reshape(experts * room, -1)
-    high = weight.astype(jnp.bfloat16)
-    low = (weight - high.astype(jnp.float32)).astype(jnp.bfloat16)
-
-    def weighted(part):
-        spread = jnp.broadcast_to(part.T[:, None, :], (experts, room, length))
-        spread = jnp.where(picked, spread.reshape(experts * room, length), 0)
-        return jnp.einsum("pt,pd->td", spread, back, preferred_element_type=jnp.float32)
-
-    routed = weighted(high) + weighted(low)
-    shared = feed_forward(normed, common_gate_weight, common_up_weight, common_down_weight)
-    return (attended.astype(jnp.float32) + shared + routed).astype(jnp.bfloat16)
+    slot = jnp.where(named, slot, float(room))
+    info = jnp.concatenate(
+        [slot.T.reshape(count, ring, length), weight.T.reshape(count, ring, length)], axis=1
+    )
+    weights = (
+        routed_gate_weight[0],
+        routed_up_weight[0],
+        routed_down_weight[0],
+        common_gate_weight,
+        common_up_weight,
+        common_down_weight,
+    )
+    return experts_part(normed, attended, info, count, ring, room, weights, 2)
 
 
 def solution(mesh):

time: 531 us -> 356 us (0.67)
  the two profiles are of different devices: /device:TPU:15 before, /device:TPU:1 now
where the time goes in v1:
time: 356 us; the launch traced here: 351 us
  Pallas kernels  259 us (73%)
  matrix products  46 us (13%)
  other arithmetic  19.6 us (6%)
  local copies, waits for them, and re-layouts  18.3 us (5%)
  blocking collectives  6.51 us (2%)
    pallas_call x1, Pallas kernels, experts_part(): pl.pallas_call(functools.partial(experts_kernel, count, ring, room, piece...  204 us
    pallas_call x2, Pallas kernels, exchange(): pl.pallas_call(functools.partial(exchange_kernel, axes, sizes), out_shape...  44 us
    dot_general x7, matrix products, shift_join(): jnp.einsum('hned,hndf->hnef', stacked[:, :-step], later[:, :, :width], pr...  15.3 us
    pallas_call x1, Pallas kernels, invert_unit_lower(): pl.pallas_call(invert_kernel, grid=(number // group,), out_shape=jax.Shap...  11.1 us
    dot_general x1, matrix products, mix_heads(): maps = jnp.einsum('hnce,hncd->hned', solved, k_decayed, precision=HIGH)  7.92 us

profile of v1, /device:TPU:1, one launch (start us, length us, event | category | flops | bytes accessed | tf_op | source)
XLA Modules:
  0.0 350.8 jit_solution(7398215578252759254)
XLA Ops:
  1.5 0.9 reduce_window_sum.11
  2.7 1.4 fusion.85
  6.4 3.7 %fusion.36 = f32[4,8,64,64]{3,2,1,0:T(8,128)} fusion(f32[8,64,4,128]{3,2,1,0:T(4,128)S(1)} %reshape.150, f32[4,8,64]{2,1,0:T(8,128)S(1)} %bitcast.147, f32[4,8,64]{2,1,0:T(8,128)S(1)} %reduce_window_sum.11, f32[8,64,4]{1,0,2:T(8,128)S(1)} %copy.47, pred[64,64]{1,0:T(8,128)(4,1)S(1)} %get-tuple-element.27, pred[64,64]{1,0:T(8,128)(4,1)S(1)} %get-tuple-element.28), kind=kOutput, calls=%fused_computation.49 | convolution fusion | flops 202768384 | bytes 1605632 | tf_op jit(solution)/shard_map/hncd,hnsd->hncs/dot_general | solution.py:199
  10.1 11.1 %shard_map.190 = f32[32,64,64]{2,1,0:T(8,128)} custom-call(f32[32,64,64]{2,1,0:T(8,128)} %bitcast.141), custom_call_target="tpu_custom_call" | custom-call | tf_op jit(solution)/shard_map/pallas_call | solution.py:145
  22.4 1.9 fusion.10
  24.4 7.9 %fusion.61 = f32[4,8,256,128]{3,2,1,0:T(8,128)S(1)} fusion(f32[4,8,64,256]{3,2,1,0:T(8,128)S(1)} %fusion.10, f32[8,64,4,128]{3,2,1,0:T(4,128)S(1)} %reshape.150, f32[4,8,64]{2,1,0:T(8,128)S(1)} %get-tuple-element.19, f32[8,64,4]{1,0,2:T(8,128)S(1)} %copy.47), kind=kOutput, calls=%fused_computation.94 | convolution fusion | flops 805830656 | bytes 7356416 | tf_op jit(solution)/shard_map/hnce,hncd->hned/dot_general | solution.py:216
  32.8 4.3 %fusion.2 = f32[4,7,256,128]{3,2,1,0:T(8,128)S(1)} fusion(f32[4,8,128,128]{3,2,1,0:T(8,128)S(1)} %get-tuple-element.6, f32[4,8,128,128]{3,2,1,0:T(8,128)S(1)} %get-tuple-element.5), kind=kOutput, calls=%fused_computation.10 | convolution fusion | flops 1410334720 | bytes 9699328 | tf_op jit(solution)/shard_map/hned,hndf->hnef/dot_general | solution.py:84
  38.1 3.0 fusion.21
  42.2 2.0 fusion.4
  45.8 1.2 pad_maximum_fusion.7.x_ref
  46.9 27.1 %shard_map.191 = f32[16,160,128]{2,1,0:T(8,128)} custom-call(f32[16,160,128]{2,1,0:T(8,128)} %pad_maximum_fusion.7.x_ref), custom_call_target="tpu_custom_call" | custom-call | tf_op jit(solution)/shard_map/pallas_call | solution.py:67
  74.1 2.9 convolution_bitcast_fusion
  77.0 1.0 slice_add_fusion.4
  78.0 0.9 slice.271
  78.9 1.2 convolution_bitcast_fusion.1
  80.4 1.1 convolution_bitcast_fusion.2
  84.4 2.3 fusion.5
  87.4 16.8 %shard_map.192 = f32[16,32,128]{2,1,0:T(8,128)} custom-call(f32[16,32,128]{2,1,0:T(8,128)} %concatenate.76.x_ref), custom_call_target="tpu_custom_call" | custom-call | tf_op jit(solution)/shard_map/pallas_call | solution.py:67
  104.2 2.7 fusion.84
  107.0 2.6 mul.163
  109.5 1.9 reduce_sum.45
  112.1 1.1 copy.45
  113.2 2.5 reshape.149
  115.8 3.4 convolution_multiply_fusion
  119.1 1.9 fusion.90
  121.1 3.9 %slice_add_fusion = f32[4,7,128,128]{3,2,1,0:T(8,128)S(1)} fusion(f32[4,8,256,128]{3,2,1,0:T(8,128)} %fusion.5, f32[4,128,128,1]{2,1,3,0:T(8,128)S(1)} %bitcast.134), kind=kOutput, calls=%fused_computation.32 | convolution fusion | flops 705101824 | bytes 5767168 | tf_op jit(solution)/shard_map/hed,hndf->hnef/dot_general | solution.py:229
  125.0 4.3 %multiply_reduce_fusion = (f32[8,64,4]{1,0,2:T(8,128)S(1)}, f32[8,64,4,128]{3,1,0,2:T(8,128)S(1)}) fusion(f32[4,7,128,128]{3,2,1,0:T(8,128)S(1)} %slice_add_fusion, f32[4,1,128,128]{3,2,1,0:T(8,128)S(1)} %bitcast.135, f32[4,8,64,256]{3,2,1,0:T(8,128)S(1)} %fusion.90, f32[8,64,4,128]{3,2,1,0:T(4,128)S(1)} %copy-done.6, ...), kind=kOutput, calls=%fused_computation.99 | convolution fusion | flops 404748288 | bytes 6316032 | tf_op jit(solution)/shard_map/hncd,hned->hnce/dot_general | solution.py:231
  131.4 6.5 %all_to_all.19 = bf16[2,256,512]{1,2,0:T(8,128)(2,1)S(1)} all-to-all(bf16[2,256,512]{1,2,0:T(8,128)(2,1)S(1)} %copy.55), channel_id=1, replica_groups=mesh['sp'=16,'tp'=2] {'tp'}, dimensions={0} | all-to-all | bytes 1048576 | tf_op jit(solution)/shard_map/all_to_all | solution.py:787
  138.0 3.6 %fusion.7 = (f32[256]{0:T(256)S(1)}, bf16[256,2048]{1,0:T(8,128)(2,1)S(1)}) fusion(bf16[256,1024]{0,1:T(8,128)(2,1)S(1)} %bitcast.145, bf16[1024,2048]{1,0:T(8,128)(2,1)} %param.29, bf16[256,2048]{1,0:T(8,128)(2,1)S(1)} %copy-done.21), kind=kOutput, calls=%fused_computation.20 | convolution fusion | flops 1076887296 | bytes 6816768 | tf_op jit(solution)/shard_map/dot_general | solution.py:788
  142.6 1.3 fusion.9.x_ref
  143.9 204.4 %experts.1 = bf16[256,2048]{1,0:T(8,128)(2,1)} custom-call(bf16[256,2048]{1,0:T(8,128)(2,1)} %fusion.9.x_ref, bf16[256,2048]{1,0:T(8,128)(2,1)} %copy-done.12, f32[4,16,256]{2,1,0:T(8,128)} %pad_maximum_fusion.16.info_ref, bf16[2048,512]{1,0:T(8,128)(2,1)} %bitcast.136, bf16[2048,512]{1,0:T(8,128)(2,1)} %bitcast.137, bf16[512,2048]{1,0:T(8,128)(2,1)} %bitcast.138, ...), custom_call_target="tpu_custom_call" | custom-call | tf_op jit(solution)/shard_map/experts/pallas_call | solution.py:715
  348.3 2.3 copy.93
  (97 shorter events, 16.9 us)
Async XLA Ops:
  4.5 1.2 copy-start.18
  4.5 1.3 copy-start.14
  21.2 1.2 copy-start.11
  41.2 1.0 copy-start.9
  41.6 2.6 copy-start
  41.6 2.6 copy-start.7
  44.4 1.0 copy-start.2
  44.5 1.3 copy-start.4
  81.5 1.2 copy-start.10
  81.6 1.5 copy-start.5
  81.6 2.0 copy-start.8
  81.7 2.4 copy-start.1
  81.7 2.7 copy-start.3
  119.1 2.0 copy-start.13
  121.1 4.0 %copy-start.6 = (f32[8,64,4,128]{3,2,1,0:T(4,128)S(1)}, f32[8,64,4,128]{3,2,1,0:T(4,128)}, u32[]{:S(2)}) copy-start(f32[8,64,4,128]{3,2,1,0:T(4,128)} %reshape.149) | copy-start | bytes 3145732
  129.3 0.9 copy-start.20
  129.3 1.5 copy-start.15
  130.8 7.1 %copy-start.21 = (bf16[256,2048]{1,0:T(8,128)(2,1)S(1)}, bf16[256,2048]{1,0:T(8,128)(2,1)}, u32[]{:S(2)}) copy-start(bf16[256,2048]{1,0:T(8,128)(2,1)} %param.30) | copy-start | bytes 3145732
  138.0 3.7 %copy-start.16 = (s32[256,4]{0,1:T(4,128)S(1)}, s32[256,4]{0,1:T(4,128)}, u32[]{:S(2)}) copy-start(s32[256,4]{0,1:T(4,128)} %param.32) | copy-start | bytes 12292
  138.0 3.9 %copy-start.19 = (f32[256,4]{0,1:T(4,128)S(1)}, f32[256,4]{0,1:T(4,128)}, u32[]{:S(2)}) copy-start(f32[256,4]{0,1:T(4,128)} %param.33) | copy-start | bytes 12292
  138.0 4.7 %copy-start.17 = (f32[2048]{0:T(1024)S(1)}, f32[2048]{0:T(1024)}, u32[]{:S(2)}) copy-start(f32[2048]{0:T(1024)} %param.31) | copy-start | bytes 24580
  141.6 1.0 copy-start.12

commit v2 on v1

--- a/solution.py
+++ b/solution.py
@@ -15,239 +15,421 @@
 HIGH = lax.Precision.HIGHEST
 
 
-def exchange_kernel(axes, sizes, x_ref, o_ref, held, send_sem, recv_sem, local_sem):
-    count = 1
-    me = 0
-    for axis, size in zip(axes, sizes):
-        count *= size
-        me = me * size + lax.axis_index(axis)
-
-    def device(index):
-        found = {}
-        for axis, size in reversed(list(zip(axes, sizes))):
-            found[axis] = lax.rem(index, size)
-            index = index // size
-        return found
+def halves(x):
+    high = x.astype(jnp.bfloat16)
+    return high, (x - high.astype(jnp.float32)).astype(jnp.bfloat16)
+
+
+NN = (((1,), (0,)), ((), ()))
+NT = (((1,), (1,)), ((), ()))
+
+
+def once(a, b, dims=NN):
+    return lax.dot_general(
+        a.astype(jnp.bfloat16), b.astype(jnp.bfloat16), dims, preferred_element_type=jnp.float32
+    )
+
+
+def thrice(a, b, dims=NN):
+    a_high, a_low = halves(a)
+    b_high, b_low = halves(b)
+
+    def dot(x, y):
+        return lax.dot_general(x, y, dims, preferred_element_type=jnp.float32)
+
+    return dot(a_high, b_high) + (dot(a_high, b_low) + dot(a_low, b_high))
+
+
+def silu(x):
+    return x * jax.nn.sigmoid(x)
+
+
+def heads_kernel(
+    count,
+    span,
+    q_ref,
+    k_ref,
+    v_ref,
+    gate_ref,
+    small_ref,
+    gain_ref,
+    residual_ref,
+    mixture_gain_ref,
+    matrix_hbm,
+    normed_ref,
+    attended_ref,
+    erase,
+    fresh,
+    score,
+    reads,
+    late,
+    maps,
+    fade,
+    gathered,
+    prefix,
+    carried,
+    starting,
+    start,
+    mixed,
+    finished,
+    token_heads,
+    matrix,
+    matrix_sem,
+    ring_send,
+    ring_recv,
+    line_send,
+    line_recv,
+    home_send,
+    home_recv,
+    pair_send,
+    pair_recv,
+):
+    f32 = jnp.float32
+    length, columns = q_ref.shape
+    heads, number = erase.shape[:2]
+    width = columns // heads
+    tp_size = lax.axis_size("tp")
+    members = lax.axis_size("sp") // count
+    parts = members // heads
+    slab = width // parts
+    sp = lax.axis_index("sp")
+    tp = lax.axis_index("tp")
+    outer = sp // members
+    member = lax.rem(sp, members)
+    MESH = pl.DeviceIdType.MESH
+    own = length // tp_size
+
+    load = pltpu.make_async_copy(matrix_hbm, matrix, matrix_sem)
+    load.start()
+
+    def device(o, m, t):
+        return {"sp": o * members + m, "tp": t}
 
     barrier = pltpu.get_barrier_semaphore()
+
+    def greet(where):
+        pl.semaphore_signal(barrier, inc=1, device_id=where, device_id_type=MESH)
+
     for step in range(1, count):
-        pl.semaphore_signal(
-            barrier,
-            inc=1,
-            device_id=device(lax.rem(me + step, count)),
-            device_id_type=pl.DeviceIdType.MESH,
-        )
-    pl.semaphore_wait(barrier, count - 1)
-    copies = []
-    for step in range(1, count):
-        peer = lax.rem(me + step, count)
-        copy = pltpu.make_async_remote_copy(
-            src_ref=x_ref.at[peer],
-            dst_ref=o_ref.at[me],
-            send_sem=send_sem.at[step],
-            recv_sem=recv_sem.at[step],
-            device_id=device(peer),
-            device_id_type=pl.DeviceIdType.MESH,
-        )
-        copy.start()
-        copies.append(copy)
-    into = pltpu.make_async_copy(x_ref.at[me], held, local_sem)
-    into.start()
-    into.wait()
-    out = pltpu.make_async_copy(held, o_ref.at[me], local_sem)
-    out.start()
-    out.wait()
-    for copy in copies:
-        copy.wait()
-
-
-def exchange(value, axes, identity):
-    sizes = tuple(lax.axis_size(axis) for axis in axes)
-    count = value.shape[0]
-    return pl.pallas_call(
-        functools.partial(exchange_kernel, axes, sizes),
-        out_shape=jax.ShapeDtypeStruct(value.shape, value.dtype),
-        in_specs=[pl.BlockSpec(memory_space=pl.ANY)],
-        out_specs=pl.BlockSpec(memory_space=pl.ANY),
-        scratch_shapes=[
-            pltpu.VMEM(value.shape[1:], value.dtype),
-            pltpu.SemaphoreType.DMA((count,)),
-            pltpu.SemaphoreType.DMA((count,)),
-            pltpu.SemaphoreType.DMA,
-        ],
-        compiler_params=pltpu.CompilerParams(collective_id=identity, has_side_effects=True),
-    )(value)
-
-
-def shift_join(stacked, step, width):
-    later = stacked[:, step:]
-    joined = jnp.einsum(
-        "hned,hndf->hnef", stacked[:, :-step], later[:, :, :width], precision=HIGH
-    )
-    joined = jnp.concatenate(
-        [joined[:, :, :width], joined[:, :, width:] + later[:, :, width:]], axis=2
-    )
-    return jnp.concatenate([stacked[:, :step], joined], axis=1)
-
-
-def inclusive(stacked, width):
-    step = 1
-    while step < stacked.shape[1]:
-        stacked = shift_join(stacked, step, width)
-        step *= 2
-    return stacked
-
-
-def starts_of(total):
-    heads, _, width = total.shape
-    count = lax.axis_size("sp")
-    parts = count // heads
-    mapping = jnp.repeat(total[:, :width], parts, axis=0)
-    carried = total[:, width:].reshape(count, width // parts, width)
-    arrived = exchange(jnp.concatenate([mapping, carried], axis=1), ("sp",), 0)
-    joined = inclusive(arrived[None], width)[0, :, width:]
-    before = jnp.concatenate([jnp.zeros_like(joined[:1]), joined[:-1]], axis=0)
-    return exchange(before, ("sp",), 1).reshape(heads, width, width)
-
-
-def invert_kernel(n_ref, x_ref):
-    span = n_ref.shape[-1]
+        greet(device(lax.rem(outer + step, count), member, tp))
+    for step in range(1, members):
+        greet(device(outer, lax.rem(member + step, members), tp))
+    for step in range(1, tp_size):
+        greet(device(outer, member, lax.rem(tp + step, tp_size)))
+
     row = lax.broadcasted_iota(jnp.int32, (span, span), 0)
     column = lax.broadcasted_iota(jnp.int32, (span, span), 1)
-    one = (row == column).astype(jnp.float32)
-    strict = [n_ref[i] for i in range(n_ref.shape[0])]
-    found = None
-    size = 1
-    while size < span:
-        pair = (row // size) - (column // size)
-        mask = ((row // size) % 2 == 1) & (pair == 1)
-        below = [jnp.where(mask, part, 0.0) for part in strict]
-        if found is None:
-            found = [one - part for part in below]
-        else:
-            inner = [
-                jnp.dot(x, part, precision=HIGH, preferred_element_type=jnp.float32)
-                for x, part in zip(found, below)
-            ]
-            found = [
-                x - jnp.dot(y, x, precision=HIGH, preferred_element_type=jnp.float32)
-                for x, y in zip(found, inner)
-            ]
-        size *= 2
-    for i, x in enumerate(found):
-        x_ref[i] = x
-
-
-def invert_unit_lower(strict):
-    number, span, _ = strict.shape
-    group = 8 if number % 8 == 0 else 1
-    spec = pl.BlockSpec((group, span, span), lambda i: (i, 0, 0))
+    causal = row >= column
+    strict = row > column
+    one = (row == column).astype(f32)
+    lower = causal.astype(f32)
+    group = 2 if number % 2 == 0 else 1
+
+    def prepare(it, carry):
+        jobs = []
+        for part in range(group):
+            c = it * group + part
+            rows = pl.ds(pl.multiple_of(c * span, span), span)
+            small = small_ref[rows, :]
+            summed = jnp.dot(
+                lower, small, precision=HIGH, preferred_element_type=f32
+            )
+            turned = summed.T
+            for h in range(heads):
+                cols = slice(h * width, (h + 1) * width)
+                q = silu(q_ref[rows, cols].astype(f32))
+                q = q * lax.rsqrt(jnp.sum(q * q, axis=-1, keepdims=True) + EPS)
+                k = silu(k_ref[rows, cols].astype(f32))
+                k = k * lax.rsqrt(jnp.sum(k * k, axis=-1, keepdims=True) + EPS)
+                beta = small[:, h : h + 1]
+                g_column = summed[:, heads + h : heads + h + 1]
+                g_row = turned[heads + h : heads + h + 1, :]
+                decay = jnp.where(
+                    causal, jnp.exp(jnp.where(causal, g_column - g_row, 0.0)), 0.0
+                )
+                kb = k * beta
+                both = thrice(jnp.concatenate([kb, q], axis=0), k, NT)
+                below = jnp.where(strict, both[:span] * decay, 0.0)
+                score[h, c] = both[span:] * decay
+                grown = jnp.exp(g_column)
+                reads[h, c] = q * grown
+                last = g_column[span - 1 :, :]
+                late[h, c] = k * jnp.exp(last - g_column)
+                fade[h, c] = jnp.broadcast_to(jnp.exp(last), fade.shape[2:])
+                v = silu(v_ref[rows, cols].astype(f32)) * beta
+                jobs.append((h, c, below, jnp.concatenate([kb * grown, v], axis=1)))
+        found = None
+        size = 1
+        while size < span:
+            pair = (row // size) - (column // size)
+            mask = ((row // size) % 2 == 1) & (pair == 1)
+            pieces = [jnp.where(mask, job[2], 0.0) for job in jobs]
+            if found is None:
+                found = [one - piece for piece in pieces]
+            else:
+                inner = [once(x, piece) for x, piece in zip(found, pieces)]
+                found = [x - once(y, x) for x, y in zip(found, inner)]
+            size *= 2
+        wrong = [one - x - thrice(job[2], x) for x, job in zip(found, jobs)]
+        found = [x + once(x, e) for x, e in zip(found, wrong)]
+        for x, (h, c, _, right) in zip(found, jobs):
+            solved = thrice(x, right)
+            erase[h, c] = solved[:, :width]
+            fresh[h, c] = solved[:, width:].T
+        return carry
+
+    lax.fori_loop(0, number // group, prepare, 0)
+
+    square = (
+        lax.broadcasted_iota(jnp.int32, (width, width), 0)
+        == lax.broadcasted_iota(jnp.int32, (width, width), 1)
+    ).astype(f32)
+    for h in range(heads):
+        maps[h, pl.ds(0, width), :] = square
+        maps[h, pl.ds(width, width), :] = jnp.zeros((width, width), f32)
+
+    def advance(c, carry):
+        rows = pl.ds(pl.multiple_of(c * span, span), span)
+        for h in range(heads):
+            state = maps[h]
+            gone = thrice(state, erase[h, c], NT)
+            news = jnp.concatenate([-gone[:width], fresh[h, c] - gone[width:]], axis=0)
+            mixed[h, rows, :] = thrice(reads[h, c], state, NT) + thrice(score[h, c], news, NT)
+            maps[h] = state * fade[h, c, 0:1, :] + thrice(news, late[h, c])
+        return carry
+
+    lax.fori_loop(0, number, advance, 0)
+
+    pl.semaphore_wait(barrier, count + members + tp_size - 3)
+
+    def remote(src, dst, send, recv, where):
+        return pltpu.make_async_remote_copy(
+            src_ref=src,
+            dst_ref=dst,
+            send_sem=send,
+            recv_sem=recv,
+            device_id=where,
+            device_id_type=MESH,
+        )
+
+    def ring_copies(step):
+        peer = lax.rem(member + step, members)
+        head = peer // parts
+        which = lax.rem(peer, parts)
+        where = device(outer, peer, tp)
+        return (
+            remote(
+                maps.at[head, pl.ds(0, width)],
+                gathered.at[member, pl.ds(0, width)],
+                ring_send.at[step, 0],
+                ring_recv.at[step, 0],
+                where,
+            ),
+            remote(
+                maps.at[head, pl.ds(pl.multiple_of(width + which * slab, slab), slab)],
+                gathered.at[member, pl.ds(width, slab)],
+                ring_send.at[step, 1],
+                ring_recv.at[step, 1],
+                where,
+            ),
+        )
+
+    for step in range(1, members):
+        for copy in ring_copies(step):
+            copy.start()
+    my_head = member // parts
+    my_part = lax.rem(member, parts)
+    gathered[member, pl.ds(0, width), :] = maps[my_head, pl.ds(0, width), :]
+    gathered[member, pl.ds(width, slab), :] = maps[
+        my_head, pl.ds(pl.multiple_of(width + my_part * slab, slab), slab), :
+    ]
+    for step in range(1, members):
+        for copy in ring_copies(step):
+            copy.wait_recv()
+
+    prefix[0, pl.ds(0, width), :] = square
+    prefix[0, pl.ds(width, slab), :] = jnp.zeros((slab, width), f32)
+    for r in range(members):
+        joined = thrice(prefix[r], gathered[r, pl.ds(0, width), :])
+        prefix[r + 1, pl.ds(0, width), :] = joined[:width]
+        prefix[r + 1, pl.ds(width, slab), :] = joined[width:] + gathered[r, pl.ds(width, slab), :]
+
+    def line_copy():
+        return remote(
+            carried.at[1],
+            carried.at[0],
+            line_send,
+            line_recv,
+            device(lax.rem(outer + 1, count), member, tp),
+        )
+
+    @pl.when(outer == 0)
+    def _():
+        carried[0] = jnp.zeros((slab, width), f32)
+
+    @pl.when(outer > 0)
+    def _():
+        line_copy().wait_recv()
+
+    arrived = carried[0]
+    carried[1] = (
+        thrice(arrived, prefix[members, pl.ds(0, width), :])
+        + prefix[members, pl.ds(width, slab), :]
+    )
+
+    @pl.when(outer + 1 < count)
+    def _():
+        line_copy().start()
+
+    for r in range(members):
+        starting[r] = (
+            thrice(arrived, prefix[r, pl.ds(0, width), :]) + prefix[r, pl.ds(width, slab), :]
+        )
+
+    def home_copy(step):
+        peer = lax.rem(member + step, members)
+        return remote(
+            starting.at[peer],
+            start.at[my_head, pl.ds(pl.multiple_of(my_part * slab, slab), slab)],
+            home_send.at[step],
+            home_recv.at[step],
+            device(outer, peer, tp),
+        )
+
+    def home_landed(step):
+        peer = lax.rem(member + members - step, members)
+        return remote(
+            starting.at[0],
+            start.at[peer // parts, pl.ds(pl.multiple_of(lax.rem(peer, parts) * slab, slab), slab)],
+            home_send.at[step],
+            home_recv.at[step],
+            device(outer, lax.rem(member + step, members), tp),
+        )
+
+    for step in range(1, members):
+        home_copy(step).start()
+    start[my_head, pl.ds(pl.multiple_of(my_part * slab, slab), slab), :] = starting[member]
+    for step in range(1, members):
+        home_landed(step).wait_recv()
+
+    def close(c, carry):
+        rows = pl.ds(pl.multiple_of(c * span, span), span)
+        for h in range(heads):
+            cols = slice(h * width, (h + 1) * width)
+            both = mixed[h, rows, :]
+            value = both[:, width:] + thrice(both[:, :width], start[h], NT)
+            scaled = value * lax.rsqrt(jnp.mean(value * value, axis=-1, keepdims=True) + EPS)
+            finished[rows, cols] = (
+                scaled * gain_ref[...] * silu(gate_ref[rows, cols].astype(f32))
+            ).astype(jnp.bfloat16)
+        return carry
+
+    lax.fori_loop(0, number, close, 0)
+
+    def pair_copy(step):
+        peer = lax.rem(tp + step, tp_size)
+        return remote(
+            finished.at[pl.ds(pl.multiple_of(peer * own, own), own)],
+            token_heads.at[tp],
+            pair_send.at[step],
+            pair_recv.at[step],
+            device(outer, member, peer),
+        )
+
+    for step in range(1, tp_size):
+        pair_copy(step).start()
+    token_heads[tp] = finished[pl.ds(pl.multiple_of(tp * own, own), own), :]
+    load.wait()
+    for step in range(1, tp_size):
+        pair_copy(step).wait_recv()
+
+    wide = residual_ref.shape[1]
+    tile = min(512, wide)
+    squares = jnp.zeros((own, 1), f32)
+    for n in range(wide // tile):
+        cols = slice(n * tile, (n + 1) * tile)
+        value = residual_ref[:, cols].astype(f32)
+        for t in range(tp_size):
+            value += jnp.dot(
+                token_heads[t],
+                matrix[pl.ds(t * columns, columns), cols],
+                preferred_element_type=f32,
+            )
+        rounded = value.astype(jnp.bfloat16)
+        attended_ref[:, cols] = rounded
+        again = rounded.astype(f32)
+        squares += jnp.sum(again * again, axis=-1, keepdims=True)
+    factor = lax.rsqrt(squares / wide + EPS)
+    for n in range(wide // tile):
+        cols = slice(n * tile, (n + 1) * tile)
+        normed_ref[:, cols] = (
+            attended_ref[:, cols].astype(f32) * factor * mixture_gain_ref[:, cols]
+        ).astype(jnp.bfloat16)
+
+    for step in range(1, members):
+        for copy in ring_copies(step):
+            copy.wait_send()
+        home_copy(step).wait_send()
+    for step in range(1, tp_size):
+        pair_copy(step).wait_send()
+
+    @pl.when(outer + 1 < count)
+    def _():
+        line_copy().wait_send()
+
+
+def heads_part(
+    queries, keys, values, gates, small, gain, residual, mixture_gain, matrix, heads, count, identity
+):
+    length, columns = queries.shape
+    width = columns // heads
+    own, wide = residual.shape
+    tp_size = lax.axis_size("tp")
+    members = lax.axis_size("sp") // count
+    parts = members // heads
+    slab = width // parts
+    span = min(2 * SPAN, length)
+    number = length // span
+    bf16, f32 = jnp.bfloat16, jnp.float32
+    vmem = pl.BlockSpec(memory_space=pltpu.VMEM)
+    dma = pltpu.SemaphoreType.DMA
     return pl.pallas_call(
-        invert_kernel,
-        grid=(number // group,),
-        out_shape=jax.ShapeDtypeStruct(strict.shape, jnp.float32),
-        in_specs=[spec],
-        out_specs=spec,
-    )(strict)
-
-
-def unit_heads(raw, heads):
-    active = jax.nn.silu(raw.astype(jnp.float32)).reshape(raw.shape[0], heads, -1)
-    return active * lax.rsqrt(jnp.sum(active * active, axis=-1, keepdims=True) + EPS)
-
-
-def prepare_inputs(
-    projected_queries,
-    projected_keys,
-    projected_values,
-    write_strength_logits,
-    decay_input_logits,
-    head_rate_logarithm,
-    extra_log_decay,
-):
-    heads = head_rate_logarithm.shape[0]
-    queries = unit_heads(projected_queries, heads)
-    keys = unit_heads(projected_keys, heads)
-    values = jax.nn.silu(projected_values.astype(jnp.float32)).reshape(
-        projected_values.shape[0], heads, -1
-    )
-    beta = jax.nn.sigmoid(write_strength_logits.astype(jnp.float32))
-    decay_logarithm = extra_log_decay - jnp.exp(head_rate_logarithm)[None, :] * jax.nn.softplus(
-        decay_input_logits.astype(jnp.float32) - 6.0
-    )
-    return (queries, keys, values, beta, decay_logarithm)
-
-
-def block_terms(queries, keys, values, beta, decay_logarithm):
-    length, heads, width = queries.shape
-    number = length // SPAN
-
-    def split(array):
-        return jnp.moveaxis(array.reshape(number, SPAN, heads, -1), 2, 0)
-
-    q_blocks = split(queries)
-    k_blocks = split(keys)
-    v_blocks = split(values)
-    b_blocks = split(beta[..., None])[..., 0]
-    g_cumul = jnp.cumsum(split(decay_logarithm[..., None])[..., 0], axis=-1)
-    place = jnp.arange(SPAN)
-    causal = place[:, None] >= place[None, :]
-    strict = place[:, None] > place[None, :]
-    spread = jnp.where(causal, g_cumul[..., :, None] - g_cumul[..., None, :], 0.0)
-    decay = jnp.where(causal, jnp.exp(spread), 0.0)
-    k_beta = k_blocks * b_blocks[..., None]
-    inner = jnp.einsum("hncd,hnsd->hncs", k_beta, k_blocks, precision=HIGH)
-    lower = jnp.where(strict, inner * decay, 0.0)
-    inverse = invert_unit_lower(lower.reshape(heads * number, SPAN, SPAN)).reshape(lower.shape)
-    right = jnp.concatenate(
-        [k_beta * jnp.exp(g_cumul)[..., None], v_blocks * b_blocks[..., None]], axis=-1
-    )
-    solved = jnp.einsum("hncs,hnsd->hncd", inverse, right, precision=HIGH)
-    scores = jnp.einsum("hncd,hnsd->hncs", q_blocks, k_blocks, precision=HIGH) * decay
-    q_decayed = q_blocks * jnp.exp(g_cumul)[..., None]
-    log_last = g_cumul[..., -1]
-    k_decayed = k_blocks * jnp.exp(log_last[..., None] - g_cumul)[..., None]
-    return (q_decayed, scores, solved, k_decayed, log_last)
-
-
-def mix_heads(terms):
-    q_decayed, scores, solved, k_decayed, log_last = terms
-    heads, number, span, width = q_decayed.shape
-    maps = jnp.einsum("hnce,hncd->hned", solved, k_decayed, precision=HIGH)
-    identity = jnp.eye(width, dtype=jnp.float32)
-    maps = jnp.concatenate(
-        [
-            identity * jnp.exp(log_last)[..., None, None] - maps[:, :, :width],
-            maps[:, :, width:],
+        functools.partial(heads_kernel, count, span),
+        name="heads",
+        out_shape=[jax.ShapeDtypeStruct((own, wide), bf16)] * 2,
+        in_specs=[vmem] * 8 + [pl.BlockSpec(memory_space=pl.ANY)],
+        out_specs=[vmem] * 2,
+        scratch_shapes=[
+            pltpu.VMEM((heads, number, span, width), f32),
+            pltpu.VMEM((heads, number, width, span), f32),
+            pltpu.VMEM((heads, number, span, span), f32),
+            pltpu.VMEM((heads, number, span, width), f32),
+            pltpu.VMEM((heads, number, span, width), f32),
+            pltpu.VMEM((heads, 2 * width, width), f32),
+            pltpu.VMEM((heads, number, 8, width), f32),
+            pltpu.VMEM((members, width + slab, width), f32),
+            pltpu.VMEM((members + 1, width + slab, width), f32),
+            pltpu.VMEM((2, slab, width), f32),
+            pltpu.VMEM((members, slab, width), f32),
+            pltpu.VMEM((heads, width, width), f32),
+            pltpu.VMEM((heads, length, 2 * width), f32),
+            pltpu.VMEM((length, columns), bf16),
+            pltpu.VMEM((tp_size, own, columns), bf16),
+            pltpu.VMEM(matrix.shape, matrix.dtype),
+            dma,
+            dma((members, 2)),
+            dma((members, 2)),
+            dma,
+            dma,
+            dma((members,)),
+            dma((members,)),
+            dma((tp_size,)),
+            dma((tp_size,)),
         ],
-        axis=2,
-    )
-    joined = inclusive(maps, width)
-    start = starts_of(joined[:, -1])
-    mixed = jnp.einsum("hncs,hnsd->hncd", scores, solved, precision=HIGH)
-    reads = q_decayed - mixed[..., :width]
-    later = jnp.einsum("hed,hndf->hnef", start, joined[:, :-1, :width], precision=HIGH)
-    states = jnp.concatenate([start[:, None], later + joined[:, :-1, width:]], axis=1)
-    result = mixed[..., width:] + jnp.einsum("hncd,hned->hnce", reads, states, precision=HIGH)
-    return result.transpose(1, 2, 0, 3).reshape(number * span, heads, width)
-
-
-def finish(head_mix, output_gate_values, per_head_norm_gain):
-    length, heads, width = head_mix.shape
-    scaled = head_mix * lax.rsqrt(jnp.mean(head_mix * head_mix, axis=-1, keepdims=True) + EPS)
-    gated = (
-        scaled
-        * per_head_norm_gain
-        * jax.nn.silu(output_gate_values.astype(jnp.float32).reshape(length, heads, width))
-    )
-    return gated.reshape(length, heads * width).astype(jnp.bfloat16)
-
-
-def normalize(stream, gain):
-    wide = stream.astype(jnp.float32)
-    return (wide * lax.rsqrt(jnp.mean(wide * wide, axis=-1, keepdims=True) + EPS) * gain).astype(
-        jnp.bfloat16
-    )
+        compiler_params=pltpu.CompilerParams(
+            collective_id=identity, has_side_effects=True, vmem_limit_bytes=60000000
+        ),
+    )(queries, keys, values, gates, small, gain, residual, mixture_gain, matrix)
 
 
 def lookup(table, index):
@@ -773,26 +955,32 @@
     common_up_weight,
     common_down_weight,
 ):
-    prepared_inputs = prepare_inputs(
+    heads = head_rate_logarithm.shape[0]
+    count = outer_size(lax.axis_size("sp"))
+    beta = jax.nn.sigmoid(write_strength_logits.astype(jnp.float32))
+    decay_logarithm = extra_log_decay - jnp.exp(head_rate_logarithm)[None, :] * jax.nn.softplus(
+        decay_input_logits.astype(jnp.float32) - 6.0
+    )
+    small = jnp.concatenate([beta, decay_logarithm], axis=1)
+    small = jnp.pad(small, ((0, 0), (0, 128 - 2 * heads)))
+    normed, attended = heads_part(
         projected_queries,
         projected_keys,
         projected_values,
-        write_strength_logits,
-        decay_input_logits,
-        head_rate_logarithm,
-        extra_log_decay,
+        output_gate_values,
+        small,
+        per_head_norm_gain[None, :],
+        residual,
+        mixture_norm_gain[None, :],
+        output_matrix,
+        heads,
+        count,
+        0,
     )
-    terms = block_terms(*prepared_inputs)
-    heads_out = finish(mix_heads(terms), output_gate_values, per_head_norm_gain)
-    token_heads = lax.all_to_all(heads_out, "tp", split_axis=0, concat_axis=1, tiled=True)
-    projected = jnp.dot(token_heads, output_matrix, preferred_element_type=jnp.float32)
-    attended = (residual.astype(jnp.float32) + projected).astype(jnp.bfloat16)
-    normed = normalize(attended, mixture_norm_gain)
     length = normed.shape[0]
     tp_size = lax.axis_size("tp")
     sp_size = lax.axis_size("sp")
     experts = sp_size * tp_size
-    count = outer_size(sp_size)
     ring = experts // count
     room = max(2, length * TOP_K * 3 // (2 * experts))
     room = -(-room // 16) * 16

time: 356 us -> 255 us (0.72)
  the two profiles are of different devices: /device:TPU:1 before, /device:TPU:0 now
where the time goes in v2:
time: 255 us; the launch traced here: 252 us
  Pallas kernels  246 us (96%)
  local copies, waits for them, and re-layouts  3.81 us (1%)
  other arithmetic  2.88 us (1%)
    pallas_call x1, Pallas kernels, experts_part(): pl.pallas_call(functools.partial(experts_kernel, count, ring, room, piece...  211 us
    pallas_call x1, Pallas kernels, heads_part(): pl.pallas_call(functools.partial(heads_kernel, count, span), name='heads'...  35 us

profile of v2, /device:TPU:0, one launch (start us, length us, event | category | flops | bytes accessed | tf_op | source)
XLA Modules:
  0.0 252.4 jit_solution(3078674000430077912)
XLA Ops:
  0.0 0.7 exp.11
  0.7 0.7 fusion.1
  1.4 0.8 fusion.3
  2.2 0.2 fusion
  2.3 0.7 select_reduce_fusion
  3.1 0.6 pad_maximum_fusion.info_ref
  3.7 0.1 copy.34
  3.9 0.7 pad.4.small_ref
  4.6 35.0 %heads.1 = (bf16[256,2048]{1,0:T(8,128)(2,1)}, bf16[256,2048]{1,0:T(8,128)(2,1)}) custom-call(bf16[512,512]{1,0:T(8,128)(2,1)} %q_ref.1, bf16[512,512]{1,0:T(8,128)(2,1)} %k_ref.1, bf16[512,512]{1,0:T(8,128)(2,1)} %v_ref.1, bf16[512,512]{1,0:T(8,128)(2,1)} %gate_ref.1, f32[512,128]{1,0:T(8,128)} %pad.4.small_ref, f32[1,128]{1,0:T(1,128)} %bitcast.18, ...), custom_call_target="tpu_custom_call" | custom-call | tf_op jit(solution)/shard_map/heads/pallas_call | solution.py:396
  39.6 210.5 %experts.1 = bf16[256,2048]{1,0:T(8,128)(2,1)} custom-call(bf16[256,2048]{1,0:T(8,128)(2,1)} %get-tuple-element.7.x_ref, bf16[256,2048]{1,0:T(8,128)(2,1)} %get-tuple-element.8.attended_ref, f32[4,16,256]{2,1,0:T(8,128)} %pad_maximum_fusion.info_ref, bf16[2048,512]{1,0:T(8,128)(2,1)} %bitcast.13, bf16[2048,512]{1,0:T(8,128)(2,1)} %bitcast.14, ...), custom_call_target="tpu_custom_call" | custom-call | tf_op jit(solution)/shard_map/experts/pallas_call | solution.py:897
  250.1 2.3 copy.36
  (1 shorter events, 0.0 us)

commit v3 on v2

--- a/solution.py
+++ b/solution.py
@@ -9,6 +9,8 @@
 
 TOP_K = 4
 SPAN = 64
+SPLIT = 2
+RELAYS = 8
 
 
 EPS = 1e-06
@@ -65,6 +67,9 @@
     late,
     maps,
     fade,
+    states,
+    changes,
+    scale,
     gathered,
     prefix,
     carried,
@@ -189,12 +194,12 @@
         maps[h, pl.ds(width, width), :] = jnp.zeros((width, width), f32)
 
     def advance(c, carry):
-        rows = pl.ds(pl.multiple_of(c * span, span), span)
         for h in range(heads):
             state = maps[h]
             gone = thrice(state, erase[h, c], NT)
             news = jnp.concatenate([-gone[:width], fresh[h, c] - gone[width:]], axis=0)
-            mixed[h, rows, :] = thrice(reads[h, c], state, NT) + thrice(score[h, c], news, NT)
+            states[h, c] = state
+            changes[h, c] = news
             maps[h] = state * fade[h, c, 0:1, :] + thrice(news, late[h, c])
         return carry
 
@@ -243,6 +248,18 @@
     gathered[member, pl.ds(width, slab), :] = maps[
         my_head, pl.ds(pl.multiple_of(width + my_part * slab, slab), slab), :
     ]
+
+    def local_reads(c, carry):
+        rows = pl.ds(pl.multiple_of(c * span, span), span)
+        for h in range(heads):
+            cols = slice(h * width, (h + 1) * width)
+            mixed[h, rows, :] = thrice(reads[h, c], states[h, c], NT) + thrice(
+                score[h, c], changes[h, c], NT
+            )
+            scale[rows, cols] = gain_ref[...] * silu(gate_ref[rows, cols].astype(f32))
+        return carry
+
+    lax.fori_loop(0, number, local_reads, 0)
     for step in range(1, members):
         for copy in ring_copies(step):
             copy.wait_recv()
@@ -319,9 +336,7 @@
             both = mixed[h, rows, :]
             value = both[:, width:] + thrice(both[:, :width], start[h], NT)
             scaled = value * lax.rsqrt(jnp.mean(value * value, axis=-1, keepdims=True) + EPS)
-            finished[rows, cols] = (
-                scaled * gain_ref[...] * silu(gate_ref[rows, cols].astype(f32))
-            ).astype(jnp.bfloat16)
+            finished[rows, cols] = (scaled * scale[rows, cols]).astype(jnp.bfloat16)
         return carry
 
     lax.fori_loop(0, number, close, 0)
@@ -407,6 +422,9 @@
             pltpu.VMEM((heads, number, span, width), f32),
             pltpu.VMEM((heads, 2 * width, width), f32),
             pltpu.VMEM((heads, number, 8, width), f32),
+            pltpu.VMEM((heads, number, 2 * width, width), f32),
+            pltpu.VMEM((heads, number, 2 * width, span), f32),
+            pltpu.VMEM((length, columns), f32),
             pltpu.VMEM((members, width + slab, width), f32),
             pltpu.VMEM((members + 1, width + slab, width), f32),
             pltpu.VMEM((2, slab, width), f32),
@@ -454,7 +472,8 @@
         leave.append(order)
         steps, latest = [], 0
         for d in order:
-            latest = max(latest, arrive[me].index(d) + 1)
+            upstream = me + 1 < count if d < me else me > 0
+            latest = count - 1 if upstream else max(latest, arrive[me].index(d) + 1)
             steps.append(latest)
         when.append(steps)
     return arrive, leave, when
@@ -512,6 +531,7 @@
     mine = lax.rem(sp, inner) * tp_size + lax.axis_index("tp")
     MESH = pl.DeviceIdType.MESH
     piece = length // pieces
+    step_rows = length // RELAYS
     slots = ring * room
     arrive, leave, when = relay_orders(count)
 
@@ -596,10 +616,9 @@
     def go_copy(j, source, step):
         peer = lax.rem(mine + step, ring)
         rows = pl.ds(pl.multiple_of(peer * room, room), room)
-        mine_rows = pl.ds(pl.multiple_of(mine * room, room), room)
         return remote(
             outbox.at[source, rows],
-            inbox.at[source, mine_rows],
+            inbox.at[source, pl.ds(step * room, room)],
             go_send.at[j, step],
             go_recv.at[j, step],
             outer,
@@ -607,11 +626,10 @@
         )
 
     def back_copy(j, source, step):
-        peer = lax.rem(mine + step, ring)
-        rows = pl.ds(pl.multiple_of(peer * room, room), room)
+        peer = lax.rem(mine + ring - step, ring)
         mine_rows = pl.ds(pl.multiple_of(mine * room, room), room)
         return remote(
-            inbox.at[source, rows],
+            inbox.at[source, pl.ds(step * room, room)],
             backbox.at[source, mine_rows],
             back_send.at[j, step],
             back_recv.at[j, step],
@@ -636,7 +654,7 @@
         for step in range(1, ring):
             go_copy(j, source, step).start()
         mine_rows = pl.ds(pl.multiple_of(mine * room, room), room)
-        inbox[source, mine_rows, :] = outbox[source, mine_rows, :]
+        inbox[source, pl.ds(0, room), :] = outbox[source, mine_rows, :]
 
     def feed(rows_ref, count_rows, w_gate, w_up, w_down, store):
         inside = w_gate.shape[1]
@@ -669,20 +687,28 @@
 
         lax.fori_loop(0, width // wide, second, 0)
 
-    def serve(j, source):
-        for step in range(1, ring):
-            go_copy(j, source, step).wait_recv()
-
-        def store(cols, value):
-            inbox[source, :, cols] = value.astype(jnp.bfloat16)
-
-        feed(inbox.at[source], slots, gate, up, down, store)
-
-    def send_back(j, source):
-        for step in range(1, ring):
-            back_copy(j, source, step).start()
-        mine_rows = pl.ds(pl.multiple_of(mine * room, room), room)
-        backbox[source, mine_rows, :] = inbox[source, mine_rows, :]
+    def serve(j, source, returns):
+        for part in range(SPLIT):
+            steps = range(part * ring // SPLIT, (part + 1) * ring // SPLIT)
+            rows = pl.ds(steps[0] * room, len(steps) * room)
+            for step in steps:
+                if step > 0:
+                    go_copy(j, source, step).wait_recv()
+
+            def store(cols, value):
+                inbox[source, rows, cols] = value.astype(jnp.bfloat16)
+
+            feed(inbox.at[source, rows], len(steps) * room, gate, up, down, store)
+            if returns:
+                send_back(j, source, steps)
+
+    def send_back(j, source, steps):
+        for step in steps:
+            if step > 0:
+                back_copy(j, source, step).start()
+            else:
+                mine_rows = pl.ds(pl.multiple_of(mine * room, room), room)
+                backbox[source, mine_rows, :] = inbox[source, pl.ds(0, room), :]
 
     def combine(j, source, store):
         weight = tables[source, ring:, :]
@@ -731,7 +757,7 @@
                 forward_copy(source, c).start()
 
     def relay_copy(dest, c):
-        rows = rows_of(c, piece)
+        rows = rows_of(c, step_rows)
         leftward = dest < outer
         target = jnp.where(leftward, outer - 1, outer + 1)
         landing = jnp.where(leftward & (target == dest), count, dest)
@@ -745,7 +771,7 @@
         )
 
     def landed(place, c):
-        rows = rows_of(c, piece)
+        rows = rows_of(c, step_rows)
         return remote(
             relay.at[place, rows],
             relay.at[place, rows],
@@ -757,8 +783,8 @@
 
     def pass_on(dest):
         upstream = ((dest < outer) & has_right) | ((dest > outer) & has_left)
-        for c in range(pieces):
-            rows = rows_of(c, piece)
+        for c in range(RELAYS):
+            rows = rows_of(c, step_rows)
 
             @pl.when(upstream)
             def _():
@@ -806,25 +832,40 @@
                     def _():
                         pass_on(drain[k])
 
-    for j in range(1, count):
-        if j == 2:
-            serve(1, order[1])
-            send_back(1, order[1])
-        receive(order[j])
-        spread(j, order[j])
+    last = count - 1
+    between = has_left & has_right
+    at_end = jnp.logical_not(between)
+
+    def early(j):
+        if j <= last:
+
+            @pl.when(between)
+            def _():
+                receive(order[j])
+
+    def late_receive(j):
+        @pl.when(at_end)
+        def _():
+            receive(order[j])
+
+    receive(order[1])
+    spread(1, order[1])
+    early(2)
+    for load in loads[3:]:
+        load.wait()
+    serve(0, order[0], False)
+    for j in range(1, last):
         if j == 1:
-            for load in loads[3:]:
-                load.wait()
-            serve(0, order[0])
-        if j > 2:
-            serve(j - 1, order[j - 1])
-            send_back(j - 1, order[j - 1])
-            collect(j - 2)
-    last = count - 1
-    if last == 1 or last > 1:
-        serve(last, order[last])
-        send_back(last, order[last])
-    send_back(0, order[0])
+            serve(j, order[j], True)
+        early(j + 2)
+        late_receive(j + 1)
+        spread(j + 1, order[j + 1])
+        if j < last - 1:
+            collect(j)
+        if j > 1:
+            serve(j, order[j], True)
+    serve(last, order[last], True)
+    send_back(0, order[0], range(ring))
     if last > 1:
         collect(last - 1)
     collect(last)
@@ -834,8 +875,8 @@
 
     combine(0, order[0], add)
     for side, place in ((has_left, outer), (has_right, count)):
-        for c in range(pieces):
-            rows = rows_of(c, piece)
+        for c in range(RELAYS):
+            rows = rows_of(c, step_rows)
 
             @pl.when(side)
             def _():
@@ -864,6 +905,7 @@
                 def _():
                     forward_copy(order[j], c).wait_send()
 
+            for c in range(RELAYS):
                 relay_copy(order[j], c).wait_send()
         for step in range(1, ring):
             go_copy(j, order[j], step).wait_send()
@@ -924,8 +966,8 @@
             dma((count, ring)),
             dma((count, ring)),
             dma((count, ring)),
-            dma((count, pieces)),
-            dma((count + 1, pieces)),
+            dma((count, RELAYS)),
+            dma((count + 1, RELAYS)),
         ],
         compiler_params=pltpu.CompilerParams(
             collective_id=identity, has_side_effects=True, vmem_limit_bytes=67043328

time: 255 us -> 238 us (0.933)
  Pallas kernels: 246 us -> 231 us
    pallas_call x1, Pallas kernels: 211 us -> 198 us  [experts_part(): pl.pallas_call(functools.partial(experts_kernel, count, ring, room, piece...]
where the time goes in v3:
time: 238 us
  Pallas kernels  231 us (97%)
  local copies, waits for them, and re-layouts  3.81 us (2%)
  other arithmetic  2.88 us (1%)
    pallas_call x1, Pallas kernels, experts_part(): pl.pallas_call(functools.partial(experts_kernel, count, ring, room, piece...  198 us
    pallas_call x1, Pallas kernels, heads_part(): pl.pallas_call(functools.partial(heads_kernel, count, span), name='heads'...  33.1 us

profile of v3, /device:TPU:0, one launch (start us, length us, event | category | flops | bytes accessed | tf_op | source)
XLA Modules:
  0.0 237.6 jit_solution(76855664711632880)
XLA Ops:
  0.0 0.7 exp.11
  0.7 0.7 fusion.1
  1.4 0.8 fusion.3
  2.2 0.2 fusion
  2.3 0.7 select_reduce_fusion
  3.1 0.6 pad_maximum_fusion.info_ref
  3.7 0.1 copy.34
  3.9 0.7 pad.4.small_ref
  4.6 33.1 %heads.1 = (bf16[256,2048]{1,0:T(8,128)(2,1)}, bf16[256,2048]{1,0:T(8,128)(2,1)}) custom-call(bf16[512,512]{1,0:T(8,128)(2,1)} %q_ref.1, bf16[512,512]{1,0:T(8,128)(2,1)} %k_ref.1, bf16[512,512]{1,0:T(8,128)(2,1)} %v_ref.1, bf16[512,512]{1,0:T(8,128)(2,1)} %gate_ref.1, f32[512,128]{1,0:T(8,128)} %pad.4.small_ref, f32[1,128]{1,0:T(1,128)} %bitcast.18, ...), custom_call_target="tpu_custom_call" | custom-call | tf_op jit(solution)/shard_map/heads/pallas_call | solution.py:411
  37.7 197.5 %experts.1 = bf16[256,2048]{1,0:T(8,128)(2,1)} custom-call(bf16[256,2048]{1,0:T(8,128)(2,1)} %get-tuple-element.7.x_ref, bf16[256,2048]{1,0:T(8,128)(2,1)} %get-tuple-element.8.attended_ref, f32[4,16,256]{2,1,0:T(8,128)} %pad_maximum_fusion.info_ref, bf16[2048,512]{1,0:T(8,128)(2,1)} %bitcast.13, bf16[2048,512]{1,0:T(8,128)(2,1)} %bitcast.14, ...), custom_call_target="tpu_custom_call" | custom-call | tf_op jit(solution)/shard_map/experts/pallas_call | solution.py:939
  235.3 2.3 copy.36
  (1 shorter events, 0.0 us)

commit v4 on v3

--- a/solution.py
+++ b/solution.py
@@ -153,7 +153,7 @@
                     causal, jnp.exp(jnp.where(causal, g_column - g_row, 0.0)), 0.0
                 )
                 kb = k * beta
-                both = thrice(jnp.concatenate([kb, q], axis=0), k, NT)
+                both = once(jnp.concatenate([kb, q], axis=0), k, NT)
                 below = jnp.where(strict, both[:span] * decay, 0.0)
                 score[h, c] = both[span:] * decay
                 grown = jnp.exp(g_column)
@@ -253,7 +253,7 @@
         rows = pl.ds(pl.multiple_of(c * span, span), span)
         for h in range(heads):
             cols = slice(h * width, (h + 1) * width)
-            mixed[h, rows, :] = thrice(reads[h, c], states[h, c], NT) + thrice(
+            mixed[h, rows, :] = once(reads[h, c], states[h, c], NT) + once(
                 score[h, c], changes[h, c], NT
             )
             scale[rows, cols] = gain_ref[...] * silu(gate_ref[rows, cols].astype(f32))
@@ -930,7 +930,7 @@
     length, width = normed.shape
     inside = weights[0].shape[1]
     shared = weights[3].shape[1]
-    pieces = 4
+    pieces = 2
     slots = ring * room
     bf16 = jnp.bfloat16
     vmem = pl.BlockSpec(memory_space=pltpu.VMEM)

time: 238 us -> 239 us (level)
  no operation moved by 1% of the time
where the time goes in v4:
time: 239 us; the launch traced here: 238 us
  Pallas kernels  231 us (97%)
  local copies, waits for them, and re-layouts  3.81 us (2%)
  other arithmetic  2.88 us (1%)
    pallas_call x1, Pallas kernels, experts_part(): pl.pallas_call(functools.partial(experts_kernel, count, ring, room, piece...  197 us
    pallas_call x1, Pallas kernels, heads_part(): pl.pallas_call(functools.partial(heads_kernel, count, span), name='heads'...  33.9 us

profile of v4, /device:TPU:0, one launch (start us, length us, event | category | flops | bytes accessed | tf_op | source)
XLA Modules:
  0.0 238.2 jit_solution(3591542905921962294)
XLA Ops:
  0.0 0.7 exp.11
  0.7 0.7 fusion.1
  1.4 0.8 fusion.3
  2.2 0.2 fusion
  2.3 0.7 select_reduce_fusion
  3.1 0.6 pad_maximum_fusion.info_ref
  3.7 0.1 copy.34
  3.9 0.7 pad.4.small_ref
  4.6 33.9 %heads.1 = (bf16[256,2048]{1,0:T(8,128)(2,1)}, bf16[256,2048]{1,0:T(8,128)(2,1)}) custom-call(bf16[512,512]{1,0:T(8,128)(2,1)} %q_ref.1, bf16[512,512]{1,0:T(8,128)(2,1)} %k_ref.1, bf16[512,512]{1,0:T(8,128)(2,1)} %v_ref.1, bf16[512,512]{1,0:T(8,128)(2,1)} %gate_ref.1, f32[512,128]{1,0:T(8,128)} %pad.4.small_ref, f32[1,128]{1,0:T(1,128)} %bitcast.18, ...), custom_call_target="tpu_custom_call" | custom-call | tf_op jit(solution)/shard_map/heads/pallas_call | solution.py:411
  38.5 197.4 %experts.1 = bf16[256,2048]{1,0:T(8,128)(2,1)} custom-call(bf16[256,2048]{1,0:T(8,128)(2,1)} %get-tuple-element.7.x_ref, bf16[256,2048]{1,0:T(8,128)(2,1)} %get-tuple-element.8.attended_ref, f32[4,16,256]{2,1,0:T(8,128)} %pad_maximum_fusion.info_ref, bf16[2048,512]{1,0:T(8,128)(2,1)} %bitcast.13, bf16[2048,512]{1,0:T(8,128)(2,1)} %bitcast.14, ...), custom_call_target="tpu_custom_call" | custom-call | tf_op jit(solution)/shard_map/experts/pallas_call | solution.py:939
  235.9 2.3 copy.36
  (1 shorter events, 0.0 us)
